TPU v7x, 512 devices: a whole 4x8x8 slice. The times are simulated.
512 devices in a mesh: fs: 64 (over z, y), tp: 8 (over x, core).
Axes of the slice: x: 4, y: 8, z: 8, core: 2. Of those that a mesh axis runs over, the one named last changes fastest.
Arguments:
- x_late: bfloat16 [16384, 2048], P('fs'), may hold values from -6 to 6
- x_early: bfloat16 [16384, 2048], P('fs'), may hold values from -6 to 6
- cotangent: bfloat16 [16384, 2048], P('fs'), may hold values from -16 to 16
- w_gate: bfloat16 [2048, 4096], P('fs', 'tp'), may hold values from -0.125 to 0.125
- w_up: bfloat16 [2048, 4096], P('fs', 'tp'), may hold values from -0.125 to 0.125
- w_down: bfloat16 [4096, 2048], P('tp', 'fs'), may hold values from -0.09375 to 0.09375
- conv_taps: float32 [3, 4096], replicated, may hold values from -3 to 3
- conv_bias: float32 [4096], replicated, may hold values from -3 to 3
- grad_down: float32 [4096, 2048], P('tp', 'fs'), may hold values from -60 to 60
Outputs:
- y_late: bfloat16 [16384, 2048], P('fs')
- dx_early: bfloat16 [16384, 2048], P('fs')
- grad_down_out: float32 [4096, 2048], P('tp', 'fs')
All inputs are finite; a program needn't handle non-finite values.
Results may differ from a plain program's by a relative error of at most 0.017.
Values may be sent and summed in bfloat16 or wider, within the bound.
No kernel may reach another device: no remote copies, remote signals or barrier semaphores. Data moves between devices by JAX's collectives and lax.ppermute only.
A program may use at most 128 MiB of HBM per device.

v0:
```python
import jax
import jax.numpy as jnp
from jax import lax
from jax.experimental import pallas as pl
from jax.experimental.pallas import tpu as pltpu
from jax.sharding import Mesh
from jax.sharding import PartitionSpec as P

AXES = ("z", "y", "x", "c")
FS = ("z", "y")
TP = ("x", "c")
NZ, NY, NX, NC = 8, 8, 4, 2
UNITS = 512
TOK = 256
WIDTH = 2048


def place(z, y, x, c):
    return ((z * NY + y) * NX + x) * NC + c


def split_groups(core_along_y):
    groups = []
    for x in range(NX):
        for k in range(8):
            groups.append([place(k, y, x, core_along_y) for y in range(NY)])
            groups.append([place(z, k, x, 1 - core_along_y) for z in range(NZ)])
    return groups


FIRST = split_groups(0)
SECOND = split_groups(1)


def contract_last(left, right):
    return lax.dot_general(
        left, right, (((1,), (1,)), ((), ())), preferred_element_type=jnp.float32
    )


def shift_later(field, steps):
    row = lax.broadcasted_iota(jnp.int32, field.shape, 0)
    return jnp.where(row >= steps, pltpu.roll(field, steps, 0), 0.0)


def shift_earlier(field, steps):
    rows = field.shape[0]
    row = lax.broadcasted_iota(jnp.int32, field.shape, 0)
    return jnp.where(row < rows - steps, pltpu.roll(field, rows - steps, 0), 0.0)


def conv_and_up(both, taps_ref, bias_ref):
    t0, t1, t2 = taps_ref[0:1, :], taps_ref[1:2, :], taps_ref[2:3, :]
    gate = both[:, 0:UNITS].astype(jnp.bfloat16).astype(jnp.float32)
    up = both[:, UNITS : 2 * UNITS]
    conv = bias_ref[0:1, :] + t2 * gate + t1 * shift_later(gate, 1) + t0 * shift_later(gate, 2)
    return conv, up


def sigmoid(v):
    return 1.0 / (1.0 + jnp.exp(-v))


def layer_kernel(
    stride_ref, taps_ref, bias_ref, xe_hbm, xl_hbm, cot_ref, w_hbm,
    keep_ref, give_ref, hidden_ref, w_ref, xe_ref, xl_ref, w_sems, x_sems,
):
    south = stride_ref[0] == 8

    def w_copy(a, m, part):
        p = jnp.where(south, a, m)
        j = jnp.where(south, m, a)
        rows = pl.ds((a * 8 + m) * 32, 32)
        cols = pl.ds(0, 2 * UNITS) if part == 0 else pl.ds(2 * UNITS, UNITS)
        return pltpu.make_async_copy(
            w_hbm.at[p, j, :, cols], w_ref.at[rows, cols], w_sems.at[part, a, m]
        )

    blocks = [(a, m) for a in range(8) for m in range(8)]
    xl_copy = pltpu.make_async_copy(xl_hbm, xl_ref, x_sems.at[4])

    def xe_copy(k):
        cols = pl.ds(k * 512, 512)
        return pltpu.make_async_copy(xe_hbm.at[:, cols], xe_ref.at[:, cols], x_sems.at[k])

    for a, m in blocks:
        if a % 2 == 0 and m == 0:
            xe_copy(a // 2).start()
        w_copy(a, m, 0).start()
    xl_copy.start()
    for a, m in blocks:
        w_copy(a, m, 1).start()

    def put(value, at):
        value = value.astype(jnp.bfloat16)

        @pl.when(south)
        def _():
            for k in range(NX):
                keep_ref[k, at] = value[k * 32 : (k + 1) * 32]
                give_ref[k, at] = value[128 + k * 32 : 128 + (k + 1) * 32]

        @pl.when(jnp.logical_not(south))
        def _():
            for k in range(NX):
                give_ref[k, at] = value[k * 32 : (k + 1) * 32]
                keep_ref[k, at] = value[128 + k * 32 : 128 + (k + 1) * 32]

    t0, t1, t2 = taps_ref[0:1, :], taps_ref[1:2, :], taps_ref[2:3, :]
    both = jnp.zeros((TOK, 2 * UNITS), jnp.float32)
    for k in range(4):
        xe_copy(k).wait()
        for a in (2 * k, 2 * k + 1):
            for m in range(8):
                w_copy(a, m, 0).wait()
        both = both + jnp.dot(
            xe_ref[:, k * 512 : (k + 1) * 512],
            w_ref[k * 512 : (k + 1) * 512, 0 : 2 * UNITS],
            preferred_element_type=jnp.float32,
        )
    conv, up = conv_and_up(both, taps_ref, bias_ref)
    sig = sigmoid(conv)
    act = conv * sig
    hidden_ref[...] = (act * up).astype(jnp.bfloat16)
    slope = up * sig * (1.0 + conv * (1.0 - sig))
    xl_copy.wait()
    late, late_up = conv_and_up(
        jnp.dot(xl_ref[...], w_ref[:, 0 : 2 * UNITS], preferred_element_type=jnp.float32),
        taps_ref,
        bias_ref,
    )
    late_hidden = (late * sigmoid(late) * late_up).astype(jnp.bfloat16)
    for a, m in blocks:
        w_copy(a, m, 1).wait()
    w_down = w_ref[:, 2 * UNITS : 3 * UNITS]
    dhidden = jnp.dot(cot_ref[...], w_down, preferred_element_type=jnp.float32)
    dup = (dhidden * act).astype(jnp.bfloat16)
    dconv = dhidden * slope
    dgate = t2 * dconv + t1 * shift_earlier(dconv, 1) + t0 * shift_earlier(dconv, 2)
    inward = jnp.concatenate([dgate.astype(jnp.bfloat16), dup], axis=1)
    put(contract_last(inward, w_ref[:, 0 : 2 * UNITS]), 1)
    put(contract_last(late_hidden, w_down), 0)


VMEM = pl.BlockSpec(memory_space=pltpu.VMEM)
SMEM = pl.BlockSpec(memory_space=pltpu.SMEM)
HBM = pl.BlockSpec(memory_space=pltpu.HBM)


def layer(strides, taps, bias, x_early, x_late, cot, w):
    piece = jax.ShapeDtypeStruct((NX, 2, 32, WIDTH), jnp.bfloat16)
    return pl.pallas_call(
        layer_kernel,
        out_shape=(piece, piece, jax.ShapeDtypeStruct((TOK, UNITS), jnp.bfloat16)),
        in_specs=[SMEM, VMEM, VMEM, HBM, HBM, VMEM, HBM],
        out_specs=(VMEM, VMEM, VMEM),
        scratch_shapes=[
            pltpu.VMEM((WIDTH, 3 * UNITS), jnp.bfloat16),
            pltpu.VMEM((TOK, WIDTH), jnp.bfloat16),
            pltpu.VMEM((TOK, WIDTH), jnp.bfloat16),
            pltpu.SemaphoreType.DMA((2, 8, 8)),
            pltpu.SemaphoreType.DMA((5,)),
        ],
        compiler_params=pltpu.CompilerParams(vmem_limit_bytes=36 * 1024 * 1024),
        cost_estimate=pl.CostEstimate(
            flops=6_000_000_000, transcendentals=0, bytes_accessed=12_000_000
        ),
        name="layer",
    )(strides, taps, bias, x_early, x_late, cot, w)


def gradient_kernel(stride_ref, cot_t_ref, hidden_ref, grad_ref):
    outer = stride_ref[0]
    inner = stride_ref[1]
    for k in range(8):
        part = jnp.dot(
            cot_t_ref[k * 256 : (k + 1) * 256, :],
            hidden_ref[...],
            preferred_element_type=jnp.float32,
        ).astype(jnp.bfloat16)
        for j in range(8):
            at = pl.multiple_of((k * outer + j * inner) * 32, 32)
            grad_ref[pl.ds(at, 32), :] = part[j * 32 : (j + 1) * 32, :]


def gradient(strides, cot_t, hidden):
    return pl.pallas_call(
        gradient_kernel,
        out_shape=jax.ShapeDtypeStruct((WIDTH, UNITS), jnp.bfloat16),
        in_specs=[SMEM, VMEM, VMEM],
        out_specs=VMEM,
        compiler_params=pltpu.CompilerParams(vmem_limit_bytes=16 * 1024 * 1024),
        cost_estimate=pl.CostEstimate(
            flops=1_000_000_000, transcendentals=0, bytes_accessed=4_000_000
        ),
        name="gradient",
    )(strides, cot_t, hidden)


def assemble_kernel(place_ref, mine_ref, other_ref, y_ref, dx_ref, sems):
    x = place_ref[0]
    core = place_ref[1]
    copies = []
    for who, ref in enumerate((mine_ref, other_ref)):
        half = core if who == 0 else 1 - core
        for d in range(NX):
            at = pl.multiple_of(half * 128 + lax.rem(x + NX - d, NX) * 32, 32)
            for k, out in enumerate((y_ref, dx_ref)):
                copies.append(
                    pltpu.make_async_copy(
                        ref.at[d, k], out.at[pl.ds(at, 32)], sems.at[who, d, k]
                    )
                )
    for c in copies:
        c.start()
    for c in copies:
        c.wait()


def assemble(where, mine, other):
    out = jax.ShapeDtypeStruct((TOK, WIDTH), jnp.bfloat16)
    return pl.pallas_call(
        assemble_kernel,
        out_shape=(out, out),
        in_specs=[SMEM, VMEM, VMEM],
        out_specs=(HBM, HBM),
        scratch_shapes=[pltpu.SemaphoreType.DMA((2, NX, 2))],
        compiler_params=pltpu.CompilerParams(vmem_limit_bytes=4 * 1024 * 1024),
        name="assemble",
    )(where, mine, other)


def exchanged(value):
    return lax.ppermute(value, "c", [(0, 1), (1, 0)])


def moved(value, steps):
    return lax.ppermute(value, "x", [(i, (i + steps) % NX) for i in range(NX)])


def f32_sum(pieces):
    return pieces.astype(jnp.float32).sum(axis=0).astype(jnp.bfloat16)


def shards(x_late, x_early, cotangent, w_gate, w_up, w_down, conv_taps, conv_bias, grad_down):
    core = lax.axis_index("c")
    x = lax.axis_index("x")
    offset = lax.axis_index(TP) * UNITS
    taps = lax.dynamic_slice_in_dim(conv_taps, offset, UNITS, 1)
    bias = lax.dynamic_slice_in_dim(conv_bias, offset, UNITS, 0)[None]
    mine = jnp.concatenate([w_gate, w_up, w_down.T], axis=1)
    near = lax.all_to_all(
        jnp.broadcast_to(mine[None], (8,) + mine.shape), AXES, 0, 0,
        tiled=True, axis_index_groups=FIRST,
    )
    w = lax.all_gather(near, AXES, axis_index_groups=SECOND)
    w, x_late, x_early = (
        pltpu.with_memory_space_constraint(v, pltpu.HBM) for v in (w, x_late, x_early)
    )
    strides = jnp.stack([8 - 7 * core, 1 + 7 * core]).astype(jnp.int32)
    keep, give, hidden = layer(strides, taps, bias, x_early, x_late, cotangent, w)
    grad_part = gradient(strides, cotangent.T, hidden)
    grad = lax.all_to_all(
        grad_part.reshape(8, 256, UNITS), AXES, 0, 0, tiled=True, axis_index_groups=SECOND
    )
    grad = f32_sum(grad).reshape(8, 32, UNITS)
    grad = lax.all_to_all(grad, AXES, 0, 0, tiled=True, axis_index_groups=FIRST)
    grad_down_out = grad_down + grad.astype(jnp.float32).sum(axis=0).T

    got = exchanged(give)

    def chip_piece(at):
        left = lax.dynamic_index_in_dim(keep, at, 0, keepdims=False)
        right = lax.dynamic_index_in_dim(got, at, 0, keepdims=False)
        return left.astype(jnp.float32) + right.astype(jnp.float32)

    total = chip_piece(x)
    for d in (2, 1, 3):
        sent = chip_piece(lax.rem(x + d, NX)).astype(jnp.bfloat16)
        arrived = moved(sent, d)
        total = total + arrived.astype(jnp.float32)
    total = total.astype(jnp.bfloat16)
    spread = {d: moved(total, d) for d in (2, 1, 3)}
    mine = jnp.stack([total] + [spread[d] for d in range(1, NX)])
    other = exchanged(mine)
    where = jnp.stack([x, core]).astype(jnp.int32)
    y_late, dx_early = assemble(where, mine, other)
    return (y_late, dx_early, grad_down_out)


def solution(mesh):
    torus = Mesh(mesh.devices.reshape(NZ, NY, NX, NC), AXES)
    return jax.shard_map(
        shards,
        mesh=torus,
        in_specs=(
            P(FS, None),
            P(FS, None),
            P(FS, None),
            P(FS, TP),
            P(FS, TP),
            P(TP, FS),
            P(),
            P(),
            P(TP, FS),
        ),
        out_specs=(P(FS, None), P(FS, None), P(TP, FS)),
        check_vma=False,
    )
```

profile of v0, /device:TPU:1, one launch (start us, length us, event | category | flops | bytes accessed | tf_op | source)
XLA Modules:
  0.0 172.7 jit_solution(14350647839892843101)
XLA Ops:
  7.2 0.0 copy-start
  7.2 0.0 copy-start.1
  7.2 0.0 all-gather.3.cloned.1.call-start
  7.2 0.9 pad_maximum_fusion.1
  8.1 0.1 broadcast_in_dim.10
  8.2 25.7 %all_to_all.15 = bf16[8,32,1536]{2,1,0:T(8,128)(2,1)} all-to-all(bf16[8,32,1536]{2,1,0:T(8,128)(2,1)S(1)} %broadcast_in_dim.10), channel_id=1, replica_groups={{0,8,16,24,32,40,48,56},{1,65,129,193,257,321,385,449},{64,72,80,88,96,..., dimensions={0} | all-to-all | bytes 1572864 | tf_op jit(solution)/shard_map/all_to_all | solution.py:252
  33.9 0.0 all-gather.3.cloned.1.call-update
  33.9 0.0 copy-done.1
  33.9 0.5 copy.14
  34.5 0.8 dynamic_slice.32
  35.2 0.1 pad_add_fusion.1.stride_ref
  35.3 0.0 copy-done
  35.3 43.8 %all-gather.3.cloned.1.call-done = bf16[64,32,1536]{2,1,0:T(8,128)(2,1)} async-done(((bf16[8,32,1536]{2,1,0:T(8,128)(2,1)}), bf16[64,32,1536]{2,1,0:T(8,128)(2,1)}) %all-gather.3.cloned.1.call-update) | async-done | bytes 6291472 | tf_op jit(solution)/shard_map/all_gather | solution.py:256
  79.1 10.8 %layer.1 = (bf16[4,2,32,2048]{3,2,1,0:T(8,128)(2,1)S(1)}, bf16[4,2,32,2048]{3,2,1,0:T(8,128)(2,1)S(1)}, bf16[256,512]{1,0:T(8,128)(2,1)S(1)}) custom-call(s32[2]{0:T(128)S(1)} %pad_add_fusion.1.stride_ref, f32[3,512]{1,0:T(4,128)S(1)} %constant_dynamic-slice_fusion.taps_ref, f32[1,512]{1,0:T(1,128)S(1)} %bitcast.31, bf16[256,2048]{1,0:T(8,128)(2,1)} %xe_hbm.1, ...), custom_call_target="tpu_custom_call" | custom-call | flops 6000000000 | bytes 12000000 | tf_op jit(solution)/shard_map/layer/pallas_call | solution.py:152
  90.0 0.0 copy-start.2
  90.0 2.6 %gradient.1 = bf16[2048,512]{1,0:T(8,128)(2,1)} custom-call(s32[2]{0:T(128)S(1)} %pad_add_fusion.1.stride_ref, bf16[2048,256]{1,0:T(8,128)(2,1)S(1)} %bitcast.30, bf16[256,512]{1,0:T(8,128)(2,1)S(1)} %get-tuple-element.12.hidden_ref), custom_call_target="tpu_custom_call" | custom-call | flops 1000000000 | bytes 4000000 | tf_op jit(solution)/shard_map/gradient/pallas_call | solution.py:187
  92.5 0.0 copy-done.2
  92.5 0.0 copy-start.3
  92.5 4.5 %all-to-all-start.1 = ((bf16[8,256,512]{2,1,0:T(8,128)(2,1)}), bf16[8,256,512]{2,1,0:T(8,128)(2,1)}, u32[]{:S(2)}, u32[]{:S(2)}) async-start(bf16[8,256,512]{2,1,0:T(8,128)(2,1)} %bitcast.16), calls=%async_computation.1 | async-start | bytes 4194304 | tf_op jit(solution)/shard_map/all_to_all | solution.py:263
  97.0 0.0 copy-done.3
  97.0 3.9 %collective-permute-start = (bf16[4,2,32,2048]{3,2,1,0:T(8,128)(2,1)S(1)}, bf16[4,2,32,2048]{3,2,1,0:T(8,128)(2,1)S(1)}, u32[]{:S(2)}, u32[]{:S(2)}) collective-permute-start(bf16[4,2,32,2048]{3,2,1,0:T(8,128)(2,1)S(1)} %copy-done.3), channel_id=1, source_target_pairs={{0,1},{1,0},{2,3},{3,2},{4,5},{5,4},{6,7},{7,6},{8,9},{9,8},{10,11... | collective-permute-start | bytes 3145736 | tf_op jit(solution)/shard_map/ppermute | solution.py:234
  101.0 2.2 %collective-permute-done = bf16[4,2,32,2048]{3,2,1,0:T(8,128)(2,1)S(1)} collective-permute-done((bf16[4,2,32,2048]{3,2,1,0:T(8,128)(2,1)S(1)}, bf16[4,2,32,2048]{3,2,1,0:T(8,128)(2,1)S(1)}, u32[]{:S(2)}, u32[]{:S(2)}) %collective-permute-start) | collective-permute-done | bytes 1048608 | tf_op jit(solution)/shard_map/ppermute | solution.py:234
  103.3 0.3 fusion.3
  103.5 4.3 %collective-permute-start.3 = (bf16[2,32,2048]{2,1,0:T(8,128)(2,1)S(1)}, bf16[2,32,2048]{2,1,0:T(8,128)(2,1)S(1)}, u32[]{:S(2)}, u32[]{:S(2)}) collective-permute-start(bf16[2,32,2048]{2,1,0:T(8,128)(2,1)S(1)} %get-tuple-element.14), channel_id=1, source_target_pairs={{0,6},{2,0},{4,2},{6,4},{1,7},{3,1},{5,3},{7,5},{8,14},{10,8},{12,... | collective-permute-start | bytes 786440 | tf_op jit(solution)/shard_map/ppermute | solution.py:238
  107.8 1.9 %collective-permute-start.2 = (bf16[2,32,2048]{2,1,0:T(8,128)(2,1)S(1)}, bf16[2,32,2048]{2,1,0:T(8,128)(2,1)S(1)}, u32[]{:S(2)}, u32[]{:S(2)}) collective-permute-start(bf16[2,32,2048]{2,1,0:T(8,128)(2,1)S(1)} %get-tuple-element.15), channel_id=1, source_target_pairs={{0,2},{2,4},{4,6},{6,0},{1,3},{3,5},{5,7},{7,1},{8,10},{10,12},{12... | collective-permute-start | bytes 786440 | tf_op jit(solution)/shard_map/ppermute | solution.py:238
  109.8 3.7 %collective-permute-start.1 = (bf16[2,32,2048]{2,1,0:T(8,128)(2,1)S(1)}, bf16[2,32,2048]{2,1,0:T(8,128)(2,1)}, u32[]{:S(2)}, u32[]{:S(2)}) collective-permute-start(bf16[2,32,2048]{2,1,0:T(8,128)(2,1)S(1)} %get-tuple-element.13), channel_id=1, source_target_pairs={{0,4},{2,6},{4,0},{6,2},{1,5},{3,7},{5,1},{7,3},{8,12},{10,14},{12... | collective-permute-start | bytes 786440 | tf_op jit(solution)/shard_map/ppermute | solution.py:238
  113.4 0.0 collective-permute-done.3
  113.4 5.7 %collective-permute-done.2 = bf16[2,32,2048]{2,1,0:T(8,128)(2,1)S(1)} collective-permute-done((bf16[2,32,2048]{2,1,0:T(8,128)(2,1)S(1)}, bf16[2,32,2048]{2,1,0:T(8,128)(2,1)S(1)}, u32[]{:S(2)}, u32[]{:S(2)}) %collective-permute-start.2) | collective-permute-done | bytes 262176 | tf_op jit(solution)/shard_map/ppermute | solution.py:238
  119.2 3.8 %collective-permute-done.1 = bf16[2,32,2048]{2,1,0:T(8,128)(2,1)} collective-permute-done((bf16[2,32,2048]{2,1,0:T(8,128)(2,1)S(1)}, bf16[2,32,2048]{2,1,0:T(8,128)(2,1)}, u32[]{:S(2)}, u32[]{:S(2)}) %collective-permute-start.1) | collective-permute-done | bytes 262176 | tf_op jit(solution)/shard_map/ppermute | solution.py:238
  123.0 1.1 fusion.2
  124.1 1.9 %collective-permute-start.6 = (bf16[2,32,2048]{2,1,0:T(8,128)(2,1)S(1)}, bf16[2,32,2048]{2,1,0:T(8,128)(2,1)S(1)}, u32[]{:S(2)}, u32[]{:S(2)}) collective-permute-start(bf16[2,32,2048]{2,1,0:T(8,128)(2,1)S(1)} %fusion.2), channel_id=1, source_target_pairs={{0,6},{2,0},{4,2},{6,4},{1,7},{3,1},{5,3},{7,5},{8,14},{10,8},{12,... | collective-permute-start | bytes 786440 | tf_op jit(solution)/shard_map/ppermute | solution.py:238
  126.1 3.4 %collective-permute-start.5 = (bf16[2,32,2048]{2,1,0:T(8,128)(2,1)S(1)}, bf16[2,32,2048]{2,1,0:T(8,128)(2,1)S(1)}, u32[]{:S(2)}, u32[]{:S(2)}) collective-permute-start(bf16[2,32,2048]{2,1,0:T(8,128)(2,1)S(1)} %fusion.2), channel_id=1, source_target_pairs={{0,4},{2,6},{4,0},{6,2},{1,5},{3,7},{5,1},{7,3},{8,12},{10,14},{12... | collective-permute-start | bytes 786440 | tf_op jit(solution)/shard_map/ppermute | solution.py:238
  129.4 2.8 %collective-permute-start.4 = (bf16[2,32,2048]{2,1,0:T(8,128)(2,1)S(1)}, bf16[2,32,2048]{2,1,0:T(8,128)(2,1)S(1)}, u32[]{:S(2)}, u32[]{:S(2)}) collective-permute-start(bf16[2,32,2048]{2,1,0:T(8,128)(2,1)S(1)} %fusion.2), channel_id=1, source_target_pairs={{0,2},{2,4},{4,6},{6,0},{1,3},{3,5},{5,7},{7,1},{8,10},{10,12},{12... | collective-permute-start | bytes 786440 | tf_op jit(solution)/shard_map/ppermute | solution.py:238
  132.2 0.0 collective-permute-done.6
  132.2 2.8 %collective-permute-done.5 = bf16[2,32,2048]{2,1,0:T(8,128)(2,1)S(1)} collective-permute-done((bf16[2,32,2048]{2,1,0:T(8,128)(2,1)S(1)}, bf16[2,32,2048]{2,1,0:T(8,128)(2,1)S(1)}, u32[]{:S(2)}, u32[]{:S(2)}) %collective-permute-start.5) | collective-permute-done | bytes 262176 | tf_op jit(solution)/shard_map/ppermute | solution.py:238
  135.0 7.4 %collective-permute-done.4 = bf16[2,32,2048]{2,1,0:T(8,128)(2,1)S(1)} collective-permute-done((bf16[2,32,2048]{2,1,0:T(8,128)(2,1)S(1)}, bf16[2,32,2048]{2,1,0:T(8,128)(2,1)S(1)}, u32[]{:S(2)}, u32[]{:S(2)}) %collective-permute-start.4) | collective-permute-done | bytes 262176 | tf_op jit(solution)/shard_map/ppermute | solution.py:238
  142.5 0.1 pad_maximum_fusion.mine_ref
  142.6 0.0 copy-start.4
  142.6 3.4 %collective-permute-start.7 = (bf16[4,2,32,2048]{3,2,1,0:T(8,128)(2,1)S(1)}, bf16[4,2,32,2048]{3,2,1,0:T(8,128)(2,1)S(1)}, u32[]{:S(2)}, u32[]{:S(2)}) collective-permute-start(bf16[4,2,32,2048]{3,2,1,0:T(8,128)(2,1)S(1)} %pad_maximum_fusion.mine_ref), channel_id=1, source_target_pairs={{0,1},{1,0},{2,3},{3,2},{4,5},{5,4},{6,7},{7,6},{8,9},{9,8},{10,11... | collective-permute-start | bytes 3145736 | tf_op jit(solution)/shard_map/ppermute | solution.py:234
  146.0 0.0 all-to-all-done.1
  146.0 2.7 %reduce_sum.21 = bf16[256,512]{1,0:T(8,128)(2,1)} reduce(bf16[8,256,512]{2,1,0:T(8,128)(2,1)} %all-to-all-done.1, bf16[]{:T(256)} %constant.52.clone.1), dimensions={0}, to_apply=%region_0.0 | reduce | flops 917504 | bytes 2359298 | tf_op jit(solution)/shard_map/reduce_sum | solution.py:242
  148.7 6.9 %all-to-all-start.2 = ((bf16[8,32,512]{2,1,0:T(8,128)(2,1)}), bf16[8,32,512]{2,1,0:T(8,128)(2,1)S(1)}, u32[]{:S(2)}, u32[]{:S(2)}) async-start(bf16[8,32,512]{2,1,0:T(8,128)(2,1)} %bitcast.17), calls=%async_computation.2 | async-start | bytes 524288 | tf_op jit(solution)/shard_map/all_to_all | solution.py:267
  155.6 0.1 pad_add_fusion.place_ref
  155.6 0.0 collective-permute-done.7.other_ref
  155.7 2.0 %assemble.1 = (bf16[256,2048]{1,0:T(8,128)(2,1)}, bf16[256,2048]{1,0:T(8,128)(2,1)}) custom-call(s32[2]{0:T(128)S(1)} %pad_add_fusion.place_ref, bf16[4,2,32,2048]{3,2,1,0:T(8,128)(2,1)S(1)} %pad_maximum_fusion.mine_ref, bf16[4,2,32,2048]{3,2,1,0:T(8,128)(2,1)S(1)} %collective-permute-done.7.other_ref), custom_call_target="tpu_custom_call" | custom-call | tf_op jit(solution)/shard_map/assemble/pallas_call | solution.py:222
  157.6 7.6 %all-to-all-done.2 = bf16[8,32,512]{2,1,0:T(8,128)(2,1)S(1)} async-done(((bf16[8,32,512]{2,1,0:T(8,128)(2,1)}), bf16[8,32,512]{2,1,0:T(8,128)(2,1)S(1)}, u32[]{:S(2)}, u32[]{:S(2)}) %all-to-all-start.2) | async-done | bytes 262176 | tf_op jit(solution)/shard_map/all_to_all | solution.py:267
  165.2 0.0 copy-done.4
  165.2 0.6 bitcast_add_fusion.1
  (2 shorter events, 0.0 us)
Async XLA Ops:
  7.2 28.2 %copy-start = (f32[3,4096]{1,0:T(4,128)S(1)}, f32[3,4096]{1,0:T(4,128)}, u32[]{:S(2)}) copy-start(f32[3,4096]{1,0:T(4,128)} %param.15) | copy-start | bytes 147460
  7.2 26.8 %copy-start.1 = (bf16[256,2048]{1,0:T(8,128)(2,1)S(1)}, bf16[256,2048]{1,0:T(8,128)(2,1)}, u32[]{:S(2)}) copy-start(bf16[256,2048]{1,0:T(8,128)(2,1)} %cot_ref.1) | copy-start | bytes 3145732
  7.2 71.9 %all-gather.3.cloned.1.call-start = ((), (), s32[]{:S(2)}) async-start(), calls=%async_computation.3 | async-start | bytes 7077888 | tf_op jit(solution)/shard_map/all_gather | solution.py:256
  90.0 2.6 %copy-start.2 = (bf16[4,2,32,2048]{3,2,1,0:T(8,128)(2,1)}, bf16[4,2,32,2048]{3,2,1,0:T(8,128)(2,1)S(1)}, u32[]{:S(2)}) copy-start(bf16[4,2,32,2048]{3,2,1,0:T(8,128)(2,1)S(1)} %get-tuple-element.9) | copy-start | bytes 3145732
  92.5 4.5 %copy-start.3 = (bf16[4,2,32,2048]{3,2,1,0:T(8,128)(2,1)S(1)}, bf16[4,2,32,2048]{3,2,1,0:T(8,128)(2,1)}, u32[]{:S(2)}) copy-start(bf16[4,2,32,2048]{3,2,1,0:T(8,128)(2,1)} %copy-done.2) | copy-start | bytes 3145732
  92.5 53.4 %all-to-all-start.1 = ((bf16[8,256,512]{2,1,0:T(8,128)(2,1)}), bf16[8,256,512]{2,1,0:T(8,128)(2,1)}, u32[]{:S(2)}, u32[]{:S(2)}) async-start(bf16[8,256,512]{2,1,0:T(8,128)(2,1)} %bitcast.16), calls=%async_computation.1 | async-start | bytes 4194304 | tf_op jit(solution)/shard_map/all_to_all | solution.py:263
  97.0 6.2 %collective-permute-start = (bf16[4,2,32,2048]{3,2,1,0:T(8,128)(2,1)S(1)}, bf16[4,2,32,2048]{3,2,1,0:T(8,128)(2,1)S(1)}, u32[]{:S(2)}, u32[]{:S(2)}) collective-permute-start(bf16[4,2,32,2048]{3,2,1,0:T(8,128)(2,1)S(1)} %copy-done.3), channel_id=1, source_target_pairs={{0,1},{1,0},{2,3},{3,2},{4,5},{5,4},{6,7},{7,6},{8,9},{9,8},{10,11... | collective-permute-start | bytes 3145736 | tf_op jit(solution)/shard_map/ppermute | solution.py:234
  103.5 9.9 %collective-permute-start.3 = (bf16[2,32,2048]{2,1,0:T(8,128)(2,1)S(1)}, bf16[2,32,2048]{2,1,0:T(8,128)(2,1)S(1)}, u32[]{:S(2)}, u32[]{:S(2)}) collective-permute-start(bf16[2,32,2048]{2,1,0:T(8,128)(2,1)S(1)} %get-tuple-element.14), channel_id=1, source_target_pairs={{0,6},{2,0},{4,2},{6,4},{1,7},{3,1},{5,3},{7,5},{8,14},{10,8},{12,... | collective-permute-start | bytes 786440 | tf_op jit(solution)/shard_map/ppermute | solution.py:238
  107.8 11.3 %collective-permute-start.2 = (bf16[2,32,2048]{2,1,0:T(8,128)(2,1)S(1)}, bf16[2,32,2048]{2,1,0:T(8,128)(2,1)S(1)}, u32[]{:S(2)}, u32[]{:S(2)}) collective-permute-start(bf16[2,32,2048]{2,1,0:T(8,128)(2,1)S(1)} %get-tuple-element.15), channel_id=1, source_target_pairs={{0,2},{2,4},{4,6},{6,0},{1,3},{3,5},{5,7},{7,1},{8,10},{10,12},{12... | collective-permute-start | bytes 786440 | tf_op jit(solution)/shard_map/ppermute | solution.py:238
  109.8 13.2 %collective-permute-start.1 = (bf16[2,32,2048]{2,1,0:T(8,128)(2,1)S(1)}, bf16[2,32,2048]{2,1,0:T(8,128)(2,1)}, u32[]{:S(2)}, u32[]{:S(2)}) collective-permute-start(bf16[2,32,2048]{2,1,0:T(8,128)(2,1)S(1)} %get-tuple-element.13), channel_id=1, source_target_pairs={{0,4},{2,6},{4,0},{6,2},{1,5},{3,7},{5,1},{7,3},{8,12},{10,14},{12... | collective-permute-start | bytes 786440 | tf_op jit(solution)/shard_map/ppermute | solution.py:238
  124.1 8.1 %collective-permute-start.6 = (bf16[2,32,2048]{2,1,0:T(8,128)(2,1)S(1)}, bf16[2,32,2048]{2,1,0:T(8,128)(2,1)S(1)}, u32[]{:S(2)}, u32[]{:S(2)}) collective-permute-start(bf16[2,32,2048]{2,1,0:T(8,128)(2,1)S(1)} %fusion.2), channel_id=1, source_target_pairs={{0,6},{2,0},{4,2},{6,4},{1,7},{3,1},{5,3},{7,5},{8,14},{10,8},{12,... | collective-permute-start | bytes 786440 | tf_op jit(solution)/shard_map/ppermute | solution.py:238
  126.1 9.0 %collective-permute-start.5 = (bf16[2,32,2048]{2,1,0:T(8,128)(2,1)S(1)}, bf16[2,32,2048]{2,1,0:T(8,128)(2,1)S(1)}, u32[]{:S(2)}, u32[]{:S(2)}) collective-permute-start(bf16[2,32,2048]{2,1,0:T(8,128)(2,1)S(1)} %fusion.2), channel_id=1, source_target_pairs={{0,4},{2,6},{4,0},{6,2},{1,5},{3,7},{5,1},{7,3},{8,12},{10,14},{12... | collective-permute-start | bytes 786440 | tf_op jit(solution)/shard_map/ppermute | solution.py:238
  129.4 13.0 %collective-permute-start.4 = (bf16[2,32,2048]{2,1,0:T(8,128)(2,1)S(1)}, bf16[2,32,2048]{2,1,0:T(8,128)(2,1)S(1)}, u32[]{:S(2)}, u32[]{:S(2)}) collective-permute-start(bf16[2,32,2048]{2,1,0:T(8,128)(2,1)S(1)} %fusion.2), channel_id=1, source_target_pairs={{0,2},{2,4},{4,6},{6,0},{1,3},{3,5},{5,7},{7,1},{8,10},{10,12},{12... | collective-permute-start | bytes 786440 | tf_op jit(solution)/shard_map/ppermute | solution.py:238
  142.6 22.6 %copy-start.4 = (f32[512,32]{0,1:T(8,128)S(1)}, f32[512,32]{0,1:T(8,128)}, u32[]{:S(2)}) copy-start(f32[512,32]{0,1:T(8,128)} %param.17) | copy-start | bytes 196612
  142.6 13.0 %collective-permute-start.7 = (bf16[4,2,32,2048]{3,2,1,0:T(8,128)(2,1)S(1)}, bf16[4,2,32,2048]{3,2,1,0:T(8,128)(2,1)S(1)}, u32[]{:S(2)}, u32[]{:S(2)}) collective-permute-start(bf16[4,2,32,2048]{3,2,1,0:T(8,128)(2,1)S(1)} %pad_maximum_fusion.mine_ref), channel_id=1, source_target_pairs={{0,1},{1,0},{2,3},{3,2},{4,5},{5,4},{6,7},{7,6},{8,9},{9,8},{10,11... | collective-permute-start | bytes 3145736 | tf_op jit(solution)/shard_map/ppermute | solution.py:234
  148.7 16.5 %all-to-all-start.2 = ((bf16[8,32,512]{2,1,0:T(8,128)(2,1)}), bf16[8,32,512]{2,1,0:T(8,128)(2,1)S(1)}, u32[]{:S(2)}, u32[]{:S(2)}) async-start(bf16[8,32,512]{2,1,0:T(8,128)(2,1)} %bitcast.17), calls=%async_computation.2 | async-start | bytes 524288 | tf_op jit(solution)/shard_map/all_to_all | solution.py:267
Sparse Core Ops, SparseCore 0:
  34.0 45.0 all-gather.2
where the time goes:
time: 173 us
  waiting for transfers between devices  73.4 us (42%)
  starting transfers between devices  36.7 us (21%)
  blocking collectives  25.7 us (15%)
  Pallas kernels  15.4 us (9%)
  between operations  14.3 us (8%)
  other arithmetic  5.89 us (3%)
    all_gather x1, waiting for transfers between devices, shards(): w = lax.all_gather(near, AXES, axis_index_groups=SECOND)  43.8 us
    all_to_all x1, blocking collectives, shards(): lax.all_to_all(jnp.broadcast_to(mine[None], (8,) + mine.shape), AXES, 0,...  25.7 us
    ppermute x6, waiting for transfers between devices, moved(): return lax.ppermute(value, 'x', [(i, (i + steps) % NX) for i in range(NX)])  19.8 us
    ppermute x6, starting transfers between devices, moved(): return lax.ppermute(value, 'x', [(i, (i + steps) % NX) for i in range(NX)])  17.9 us
    pallas_call x1, Pallas kernels, layer(): pl.pallas_call(layer_kernel, out_shape=(piece, piece, jax.ShapeDtypeStruc...  10.8 us
    all_to_all x1, waiting for transfers between devices, shards(): grad = lax.all_to_all(grad, AXES, 0, 0, tiled=True, axis_index_groups=FIRST)  7.56 us
    ppermute x2, starting transfers between devices, exchanged(): return lax.ppermute(value, 'c', [(0, 1), (1, 0)])  7.31 us
    all_to_all x1, starting transfers between devices, shards(): grad = lax.all_to_all(grad, AXES, 0, 0, tiled=True, axis_index_groups=FIRST)  6.9 us
  transfers between devices with their start and end apart: 11, of which 7 were waited for; matrix products, arithmetic and copies ran while one was open for 3% of the time, Pallas kernels for 1%

commit v1 on v0

--- a/solution.py
+++ b/solution.py
@@ -61,12 +61,7 @@
     return 1.0 / (1.0 + jnp.exp(-v))
 
 
-def layer_kernel(
-    stride_ref, taps_ref, bias_ref, xe_hbm, xl_hbm, cot_ref, w_hbm,
-    keep_ref, give_ref, hidden_ref, w_ref, xe_ref, xl_ref, w_sems, x_sems,
-):
-    south = stride_ref[0] == 8
-
+def block_copies(south, w_hbm, w_ref, w_sems, x_hbm, x_ref, x_sems):
     def w_copy(a, m, part):
         p = jnp.where(south, a, m)
         j = jnp.where(south, m, a)
@@ -76,20 +71,74 @@
             w_hbm.at[p, j, :, cols], w_ref.at[rows, cols], w_sems.at[part, a, m]
         )
 
-    blocks = [(a, m) for a in range(8) for m in range(8)]
-    xl_copy = pltpu.make_async_copy(xl_hbm, xl_ref, x_sems.at[4])
-
-    def xe_copy(k):
+    def x_copy(k):
         cols = pl.ds(k * 512, 512)
-        return pltpu.make_async_copy(xe_hbm.at[:, cols], xe_ref.at[:, cols], x_sems.at[k])
-
-    for a, m in blocks:
-        if a % 2 == 0 and m == 0:
-            xe_copy(a // 2).start()
-        w_copy(a, m, 0).start()
-    xl_copy.start()
-    for a, m in blocks:
-        w_copy(a, m, 1).start()
+        return pltpu.make_async_copy(x_hbm.at[:, cols], x_ref.at[:, cols], x_sems.at[k])
+
+    return w_copy, x_copy
+
+
+def start_inward(w_copy, x_copy):
+    for k in range(4):
+        x_copy(k).start()
+        for a in (2 * k, 2 * k + 1):
+            for m in range(8):
+                w_copy(a, m, 0).start()
+
+
+def gate_and_up(w_copy, x_copy, w_ref, x_ref):
+    both = jnp.zeros((TOK, 2 * UNITS), jnp.float32)
+    for k in range(4):
+        x_copy(k).wait()
+        for a in (2 * k, 2 * k + 1):
+            for m in range(8):
+                w_copy(a, m, 0).wait()
+        both = both + jnp.dot(
+            x_ref[:, k * 512 : (k + 1) * 512],
+            w_ref[k * 512 : (k + 1) * 512, 0 : 2 * UNITS],
+            preferred_element_type=jnp.float32,
+        )
+    return both
+
+
+def early_kernel(
+    stride_ref, taps_ref, bias_ref, xe_hbm, cot_t_ref, w_hbm,
+    grad_ref, act_ref, slope_ref, w_ref, xe_ref, w_sems, x_sems,
+):
+    outer = stride_ref[0]
+    inner = stride_ref[1]
+    w_copy, x_copy = block_copies(outer == 8, w_hbm, w_ref, w_sems, xe_hbm, xe_ref, x_sems)
+    start_inward(w_copy, x_copy)
+    both = gate_and_up(w_copy, x_copy, w_ref, xe_ref)
+    conv, up = conv_and_up(both, taps_ref, bias_ref)
+    sig = sigmoid(conv)
+    act = conv * sig
+    act_ref[...] = act
+    slope_ref[...] = up * sig * (1.0 + conv * (1.0 - sig))
+    hidden = (act * up).astype(jnp.bfloat16)
+    for k in range(8):
+        part = jnp.dot(
+            cot_t_ref[k * 256 : (k + 1) * 256, :], hidden, preferred_element_type=jnp.float32
+        ).astype(jnp.bfloat16)
+        for j in range(8):
+            at = pl.multiple_of((k * outer + j * inner) * 32, 32)
+            grad_ref[pl.ds(at, 32), :] = part[j * 32 : (j + 1) * 32, :]
+
+
+def outputs_kernel(
+    stride_ref, taps_ref, bias_ref, xl_hbm, cot_hbm, act_hbm, slope_hbm, w_hbm,
+    keep_ref, give_ref, w_ref, xl_ref, cot_ref, act_ref, slope_ref, w_sems, x_sems,
+):
+    south = stride_ref[0] == 8
+    w_copy, x_copy = block_copies(south, w_hbm, w_ref, w_sems, xl_hbm, xl_ref, x_sems)
+    start_inward(w_copy, x_copy)
+    rest = [
+        pltpu.make_async_copy(cot_hbm, cot_ref, x_sems.at[4]),
+        pltpu.make_async_copy(act_hbm, act_ref, x_sems.at[5]),
+        pltpu.make_async_copy(slope_hbm, slope_ref, x_sems.at[6]),
+    ] + [w_copy(a, m, 1) for a in range(8) for m in range(8)]
+    for c in rest:
+        c.start()
 
     def put(value, at):
         value = value.astype(jnp.bfloat16)
@@ -107,39 +156,19 @@
                 keep_ref[k, at] = value[128 + k * 32 : 128 + (k + 1) * 32]
 
     t0, t1, t2 = taps_ref[0:1, :], taps_ref[1:2, :], taps_ref[2:3, :]
-    both = jnp.zeros((TOK, 2 * UNITS), jnp.float32)
-    for k in range(4):
-        xe_copy(k).wait()
-        for a in (2 * k, 2 * k + 1):
-            for m in range(8):
-                w_copy(a, m, 0).wait()
-        both = both + jnp.dot(
-            xe_ref[:, k * 512 : (k + 1) * 512],
-            w_ref[k * 512 : (k + 1) * 512, 0 : 2 * UNITS],
-            preferred_element_type=jnp.float32,
-        )
-    conv, up = conv_and_up(both, taps_ref, bias_ref)
-    sig = sigmoid(conv)
-    act = conv * sig
-    hidden_ref[...] = (act * up).astype(jnp.bfloat16)
-    slope = up * sig * (1.0 + conv * (1.0 - sig))
-    xl_copy.wait()
-    late, late_up = conv_and_up(
-        jnp.dot(xl_ref[...], w_ref[:, 0 : 2 * UNITS], preferred_element_type=jnp.float32),
-        taps_ref,
-        bias_ref,
-    )
+    both = gate_and_up(w_copy, x_copy, w_ref, xl_ref)
+    late, late_up = conv_and_up(both, taps_ref, bias_ref)
     late_hidden = (late * sigmoid(late) * late_up).astype(jnp.bfloat16)
-    for a, m in blocks:
-        w_copy(a, m, 1).wait()
+    for c in rest:
+        c.wait()
     w_down = w_ref[:, 2 * UNITS : 3 * UNITS]
+    put(contract_last(late_hidden, w_down), 0)
     dhidden = jnp.dot(cot_ref[...], w_down, preferred_element_type=jnp.float32)
-    dup = (dhidden * act).astype(jnp.bfloat16)
-    dconv = dhidden * slope
+    dup = (dhidden * act_ref[...]).astype(jnp.bfloat16)
+    dconv = dhidden * slope_ref[...]
     dgate = t2 * dconv + t1 * shift_earlier(dconv, 1) + t0 * shift_earlier(dconv, 2)
     inward = jnp.concatenate([dgate.astype(jnp.bfloat16), dup], axis=1)
     put(contract_last(inward, w_ref[:, 0 : 2 * UNITS]), 1)
-    put(contract_last(late_hidden, w_down), 0)
 
 
 VMEM = pl.BlockSpec(memory_space=pltpu.VMEM)
@@ -147,54 +176,54 @@
 HBM = pl.BlockSpec(memory_space=pltpu.HBM)
 
 
-def layer(strides, taps, bias, x_early, x_late, cot, w):
-    piece = jax.ShapeDtypeStruct((NX, 2, 32, WIDTH), jnp.bfloat16)
+FIELD = jax.ShapeDtypeStruct((TOK, UNITS), jnp.float32)
+W_SPACE = pltpu.VMEM((WIDTH, 3 * UNITS), jnp.bfloat16)
+X_SPACE = pltpu.VMEM((TOK, WIDTH), jnp.bfloat16)
+F_SPACE = pltpu.VMEM((TOK, UNITS), jnp.float32)
+
+
+def early(strides, taps, bias, x_early, cot_t, w):
     return pl.pallas_call(
-        layer_kernel,
-        out_shape=(piece, piece, jax.ShapeDtypeStruct((TOK, UNITS), jnp.bfloat16)),
-        in_specs=[SMEM, VMEM, VMEM, HBM, HBM, VMEM, HBM],
+        early_kernel,
+        out_shape=(jax.ShapeDtypeStruct((WIDTH, UNITS), jnp.bfloat16), FIELD, FIELD),
+        in_specs=[SMEM, VMEM, VMEM, HBM, VMEM, HBM],
         out_specs=(VMEM, VMEM, VMEM),
         scratch_shapes=[
-            pltpu.VMEM((WIDTH, 3 * UNITS), jnp.bfloat16),
-            pltpu.VMEM((TOK, WIDTH), jnp.bfloat16),
-            pltpu.VMEM((TOK, WIDTH), jnp.bfloat16),
-            pltpu.SemaphoreType.DMA((2, 8, 8)),
-            pltpu.SemaphoreType.DMA((5,)),
+            W_SPACE,
+            X_SPACE,
+            pltpu.SemaphoreType.DMA((1, 8, 8)),
+            pltpu.SemaphoreType.DMA((4,)),
         ],
         compiler_params=pltpu.CompilerParams(vmem_limit_bytes=36 * 1024 * 1024),
         cost_estimate=pl.CostEstimate(
-            flops=6_000_000_000, transcendentals=0, bytes_accessed=12_000_000
+            flops=3_000_000_000, transcendentals=0, bytes_accessed=8_000_000
         ),
-        name="layer",
-    )(strides, taps, bias, x_early, x_late, cot, w)
-
-
-def gradient_kernel(stride_ref, cot_t_ref, hidden_ref, grad_ref):
-    outer = stride_ref[0]
-    inner = stride_ref[1]
-    for k in range(8):
-        part = jnp.dot(
-            cot_t_ref[k * 256 : (k + 1) * 256, :],
-            hidden_ref[...],
-            preferred_element_type=jnp.float32,
-        ).astype(jnp.bfloat16)
-        for j in range(8):
-            at = pl.multiple_of((k * outer + j * inner) * 32, 32)
-            grad_ref[pl.ds(at, 32), :] = part[j * 32 : (j + 1) * 32, :]
-
-
-def gradient(strides, cot_t, hidden):
+        name="early",
+    )(strides, taps, bias, x_early, cot_t, w)
+
+
+def outputs(strides, taps, bias, x_late, cot, act, slope, w):
+    piece = jax.ShapeDtypeStruct((NX, 2, 32, WIDTH), jnp.bfloat16)
     return pl.pallas_call(
-        gradient_kernel,
-        out_shape=jax.ShapeDtypeStruct((WIDTH, UNITS), jnp.bfloat16),
-        in_specs=[SMEM, VMEM, VMEM],
-        out_specs=VMEM,
-        compiler_params=pltpu.CompilerParams(vmem_limit_bytes=16 * 1024 * 1024),
+        outputs_kernel,
+        out_shape=(piece, piece),
+        in_specs=[SMEM, VMEM, VMEM, HBM, HBM, HBM, HBM, HBM],
+        out_specs=(VMEM, VMEM),
+        scratch_shapes=[
+            W_SPACE,
+            X_SPACE,
+            X_SPACE,
+            F_SPACE,
+            F_SPACE,
+            pltpu.SemaphoreType.DMA((2, 8, 8)),
+            pltpu.SemaphoreType.DMA((7,)),
+        ],
+        compiler_params=pltpu.CompilerParams(vmem_limit_bytes=36 * 1024 * 1024),
         cost_estimate=pl.CostEstimate(
-            flops=1_000_000_000, transcendentals=0, bytes_accessed=4_000_000
+            flops=4_000_000_000, transcendentals=0, bytes_accessed=12_000_000
         ),
-        name="gradient",
-    )(strides, cot_t, hidden)
+        name="outputs",
+    )(strides, taps, bias, x_late, cot, act, slope, w)
 
 
 def assemble_kernel(place_ref, mine_ref, other_ref, y_ref, dx_ref, sems):
@@ -238,6 +267,10 @@
     return lax.ppermute(value, "x", [(i, (i + steps) % NX) for i in range(NX)])
 
 
+def in_hbm(*values):
+    return [pltpu.with_memory_space_constraint(v, pltpu.HBM) for v in values]
+
+
 def f32_sum(pieces):
     return pieces.astype(jnp.float32).sum(axis=0).astype(jnp.bfloat16)
 
@@ -254,12 +287,11 @@
         tiled=True, axis_index_groups=FIRST,
     )
     w = lax.all_gather(near, AXES, axis_index_groups=SECOND)
-    w, x_late, x_early = (
-        pltpu.with_memory_space_constraint(v, pltpu.HBM) for v in (w, x_late, x_early)
-    )
     strides = jnp.stack([8 - 7 * core, 1 + 7 * core]).astype(jnp.int32)
-    keep, give, hidden = layer(strides, taps, bias, x_early, x_late, cotangent, w)
-    grad_part = gradient(strides, cotangent.T, hidden)
+    w, x_late, x_early = in_hbm(w, x_late, x_early)
+    grad_part, act, slope = early(strides, taps, bias, x_early, cotangent.T, w)
+    cot, act, slope = in_hbm(cotangent, act, slope)
+    keep, give = outputs(strides, taps, bias, x_late, cot, act, slope, w)
     grad = lax.all_to_all(
         grad_part.reshape(8, 256, UNITS), AXES, 0, 0, tiled=True, axis_index_groups=SECOND
     )

time: 173 us -> 176 us (1.017)
  waiting for transfers between devices: 73.4 us -> 66.6 us
  starting transfers between devices: 36.7 us -> 41.1 us
  Pallas kernels: 15.4 us -> 18.8 us
    ppermute x6, waiting for transfers between devices: 19.8 us -> 13 us  [moved(): return lax.ppermute(value, 'x', [(i, (i + steps) % NX) for i in range(NX)])]
    ppermute x6, starting transfers between devices: 17.9 us -> 21.8 us  [moved(): return lax.ppermute(value, 'x', [(i, (i + steps) % NX) for i in range(NX)])]
    pallas_call x2, Pallas kernels: 13.4 us -> 16.8 us  [the longest x1 9.53 us: outputs(): pl.pallas_call(outputs_kernel, out_shape=(piece, piece), in_specs=[SMEM,...]
  transfers between devices with their start and end apart: 11 -> 11, of which waited for: 7 -> 6; matrix products, arithmetic and copies ran while one was open for 3% -> 3% of each run, Pallas kernels for 1% -> 7%
where the time goes in v1:
time: 176 us; the launch traced here: 175 us
  waiting for transfers between devices  66.6 us (38%)
  starting transfers between devices  41.1 us (23%)
  blocking collectives  25.7 us (15%)
  Pallas kernels  18.8 us (11%)
  between operations  14.3 us (8%)
  other arithmetic  5.89 us (3%)
  local copies, waits for them, and re-layouts  2.95 us (2%)
    all_gather x1, waiting for transfers between devices, shards(): w = lax.all_gather(near, AXES, axis_index_groups=SECOND)  43.8 us
    all_to_all x1, blocking collectives, shards(): lax.all_to_all(jnp.broadcast_to(mine[None], (8,) + mine.shape), AXES, 0,...  25.7 us
    ppermute x6, starting transfers between devices, moved(): return lax.ppermute(value, 'x', [(i, (i + steps) % NX) for i in range(NX)])  21.8 us
    ppermute x6, waiting for transfers between devices, moved(): return lax.ppermute(value, 'x', [(i, (i + steps) % NX) for i in range(NX)])  13 us
    pallas_call x1, Pallas kernels, outputs(): pl.pallas_call(outputs_kernel, out_shape=(piece, piece), in_specs=[SMEM,...  9.53 us
    ppermute x2, starting transfers between devices, exchanged(): return lax.ppermute(value, 'c', [(0, 1), (1, 0)])  8.03 us
    all_to_all x1, waiting for transfers between devices, shards(): grad = lax.all_to_all(grad, AXES, 0, 0, tiled=True, axis_index_groups=FIRST)  7.56 us
    pallas_call x1, Pallas kernels, early(): pl.pallas_call(early_kernel, out_shape=(jax.ShapeDtypeStruct((WIDTH, UNIT...  7.27 us
  transfers between devices with their start and end apart: 11, of which 6 were waited for; matrix products, arithmetic and copies ran while one was open for 3% of the time, Pallas kernels for 7%

profile of v1, /device:TPU:1, one launch (start us, length us, event | category | flops | bytes accessed | tf_op | source)
XLA Modules:
  0.0 175.4 jit_solution(6490578787238594603)
XLA Ops:
  7.2 0.0 copy-start
  7.2 0.0 copy-start.3
  7.2 0.0 all-gather.3.cloned.1.call-start
  7.2 0.9 pad_maximum_fusion.1
  8.1 0.1 broadcast_in_dim.10
  8.2 25.7 %all_to_all.15 = bf16[8,32,1536]{2,1,0:T(8,128)(2,1)} all-to-all(bf16[8,32,1536]{2,1,0:T(8,128)(2,1)S(1)} %broadcast_in_dim.10), channel_id=1, replica_groups={{0,8,16,24,32,40,48,56},{1,65,129,193,257,321,385,449},{64,72,80,88,96,..., dimensions={0} | all-to-all | bytes 1572864 | tf_op jit(solution)/shard_map/all_to_all | solution.py:285
  33.9 0.0 all-gather.3.cloned.1.call-update
  33.9 0.0 copy-done.3
  33.9 0.5 copy.14
  34.5 0.8 dynamic_slice.32
  35.2 0.1 pad_add_fusion.1.stride_ref
  35.3 0.0 copy-done
  35.3 43.8 %all-gather.3.cloned.1.call-done = bf16[64,32,1536]{2,1,0:T(8,128)(2,1)} async-done(((bf16[8,32,1536]{2,1,0:T(8,128)(2,1)}), bf16[64,32,1536]{2,1,0:T(8,128)(2,1)}) %all-gather.3.cloned.1.call-update) | async-done | bytes 6291472 | tf_op jit(solution)/shard_map/all_gather | solution.py:289
  79.1 7.3 %early.1 = (bf16[2048,512]{1,0:T(8,128)(2,1)}, f32[256,512]{1,0:T(8,128)S(1)}, f32[256,512]{1,0:T(8,128)S(1)}) custom-call(s32[2]{0:T(128)S(1)} %pad_add_fusion.1.stride_ref, f32[3,512]{1,0:T(4,128)S(1)} %constant_dynamic-slice_fusion.taps_ref, f32[1,512]{1,0:T(1,128)S(1)} %bitcast.31, bf16[256,2048]{1,0:T(8,128)(2,1)} %xe_hbm.1, ...), custom_call_target="tpu_custom_call" | custom-call | flops 3000000000 | bytes 8000000 | tf_op jit(solution)/shard_map/early/pallas_call | solution.py:186
  86.4 0.0 copy-start.1
  86.4 0.8 copy-done.1
  87.2 0.0 copy-start.2
  87.2 0.8 copy-done.2
  88.0 4.4 %all-to-all-start.1 = ((bf16[8,256,512]{2,1,0:T(8,128)(2,1)}), bf16[8,256,512]{2,1,0:T(8,128)(2,1)}, u32[]{:S(2)}, u32[]{:S(2)}) async-start(bf16[8,256,512]{2,1,0:T(8,128)(2,1)} %bitcast.16), calls=%async_computation.1 | async-start | bytes 4194304 | tf_op jit(solution)/shard_map/all_to_all | solution.py:295
  92.3 9.5 %outputs.1 = (bf16[4,2,32,2048]{3,2,1,0:T(8,128)(2,1)S(1)}, bf16[4,2,32,2048]{3,2,1,0:T(8,128)(2,1)S(1)}) custom-call(s32[2]{0:T(128)S(1)} %pad_add_fusion.1.stride_ref, f32[3,512]{1,0:T(4,128)S(1)} %constant_dynamic-slice_fusion.taps_ref, f32[1,512]{1,0:T(1,128)S(1)} %bitcast.32, bf16[256,2048]{1,0:T(8,128)(2,1)} %xl_hbm.1, bf16[256,2048]{1,0:T(8,128)(2,1)} %cot_hbm.1, ...), custom_call_target="tpu_custom_call" | custom-call | flops 4000000000 | bytes 12000000 | tf_op jit(solution)/shard_map/outputs/pallas_call | solution.py:207
  101.9 4.0 %collective-permute-start = (bf16[4,2,32,2048]{3,2,1,0:T(8,128)(2,1)S(1)}, bf16[4,2,32,2048]{3,2,1,0:T(8,128)(2,1)S(1)}, u32[]{:S(2)}, u32[]{:S(2)}) collective-permute-start(bf16[4,2,32,2048]{3,2,1,0:T(8,128)(2,1)S(1)} %get-tuple-element.13), channel_id=1, source_target_pairs={{0,1},{1,0},{2,3},{3,2},{4,5},{5,4},{6,7},{7,6},{8,9},{9,8},{10,11... | collective-permute-start | bytes 3145736 | tf_op jit(solution)/shard_map/ppermute | solution.py:263
  105.8 2.2 %collective-permute-done = bf16[4,2,32,2048]{3,2,1,0:T(8,128)(2,1)S(1)} collective-permute-done((bf16[4,2,32,2048]{3,2,1,0:T(8,128)(2,1)S(1)}, bf16[4,2,32,2048]{3,2,1,0:T(8,128)(2,1)S(1)}, u32[]{:S(2)}, u32[]{:S(2)}) %collective-permute-start) | collective-permute-done | bytes 1048608 | tf_op jit(solution)/shard_map/ppermute | solution.py:263
  108.1 0.3 fusion.3
  108.4 4.6 %collective-permute-start.1 = (bf16[2,32,2048]{2,1,0:T(8,128)(2,1)S(1)}, bf16[2,32,2048]{2,1,0:T(8,128)(2,1)S(1)}, u32[]{:S(2)}, u32[]{:S(2)}) collective-permute-start(bf16[2,32,2048]{2,1,0:T(8,128)(2,1)S(1)} %get-tuple-element.17), channel_id=1, source_target_pairs={{0,4},{2,6},{4,0},{6,2},{1,5},{3,7},{5,1},{7,3},{8,12},{10,14},{12... | collective-permute-start | bytes 786440 | tf_op jit(solution)/shard_map/ppermute | solution.py:267
  113.0 2.2 %collective-permute-start.2 = (bf16[2,32,2048]{2,1,0:T(8,128)(2,1)S(1)}, bf16[2,32,2048]{2,1,0:T(8,128)(2,1)S(1)}, u32[]{:S(2)}, u32[]{:S(2)}) collective-permute-start(bf16[2,32,2048]{2,1,0:T(8,128)(2,1)S(1)} %get-tuple-element.19), channel_id=1, source_target_pairs={{0,2},{2,4},{4,6},{6,0},{1,3},{3,5},{5,7},{7,1},{8,10},{10,12},{12... | collective-permute-start | bytes 786440 | tf_op jit(solution)/shard_map/ppermute | solution.py:267
  115.2 4.3 %collective-permute-start.3 = (bf16[2,32,2048]{2,1,0:T(8,128)(2,1)S(1)}, bf16[2,32,2048]{2,1,0:T(8,128)(2,1)}, u32[]{:S(2)}, u32[]{:S(2)}) collective-permute-start(bf16[2,32,2048]{2,1,0:T(8,128)(2,1)S(1)} %get-tuple-element.18), channel_id=1, source_target_pairs={{0,6},{2,0},{4,2},{6,4},{1,7},{3,1},{5,3},{7,5},{8,14},{10,8},{12,... | collective-permute-start | bytes 786440 | tf_op jit(solution)/shard_map/ppermute | solution.py:267
  119.5 0.0 collective-permute-done.1
  119.5 5.9 %collective-permute-done.2 = bf16[2,32,2048]{2,1,0:T(8,128)(2,1)S(1)} collective-permute-done((bf16[2,32,2048]{2,1,0:T(8,128)(2,1)S(1)}, bf16[2,32,2048]{2,1,0:T(8,128)(2,1)S(1)}, u32[]{:S(2)}, u32[]{:S(2)}) %collective-permute-start.2) | collective-permute-done | bytes 262176 | tf_op jit(solution)/shard_map/ppermute | solution.py:267
  125.4 0.0 collective-permute-done.3
  125.4 1.1 fusion.2
  126.5 3.4 %collective-permute-start.4 = (bf16[2,32,2048]{2,1,0:T(8,128)(2,1)S(1)}, bf16[2,32,2048]{2,1,0:T(8,128)(2,1)S(1)}, u32[]{:S(2)}, u32[]{:S(2)}) collective-permute-start(bf16[2,32,2048]{2,1,0:T(8,128)(2,1)S(1)} %fusion.2), channel_id=1, source_target_pairs={{0,2},{2,4},{4,6},{6,0},{1,3},{3,5},{5,7},{7,1},{8,10},{10,12},{12... | collective-permute-start | bytes 786440 | tf_op jit(solution)/shard_map/ppermute | solution.py:267
  129.9 3.9 %collective-permute-start.5 = (bf16[2,32,2048]{2,1,0:T(8,128)(2,1)S(1)}, bf16[2,32,2048]{2,1,0:T(8,128)(2,1)S(1)}, u32[]{:S(2)}, u32[]{:S(2)}) collective-permute-start(bf16[2,32,2048]{2,1,0:T(8,128)(2,1)S(1)} %fusion.2), channel_id=1, source_target_pairs={{0,4},{2,6},{4,0},{6,2},{1,5},{3,7},{5,1},{7,3},{8,12},{10,14},{12... | collective-permute-start | bytes 786440 | tf_op jit(solution)/shard_map/ppermute | solution.py:267
  133.8 3.4 %collective-permute-start.6 = (bf16[2,32,2048]{2,1,0:T(8,128)(2,1)S(1)}, bf16[2,32,2048]{2,1,0:T(8,128)(2,1)S(1)}, u32[]{:S(2)}, u32[]{:S(2)}) collective-permute-start(bf16[2,32,2048]{2,1,0:T(8,128)(2,1)S(1)} %fusion.2), channel_id=1, source_target_pairs={{0,6},{2,0},{4,2},{6,4},{1,7},{3,1},{5,3},{7,5},{8,14},{10,8},{12,... | collective-permute-start | bytes 786440 | tf_op jit(solution)/shard_map/ppermute | solution.py:267
  137.3 0.0 collective-permute-done.4
  137.3 4.9 %collective-permute-done.5 = bf16[2,32,2048]{2,1,0:T(8,128)(2,1)S(1)} collective-permute-done((bf16[2,32,2048]{2,1,0:T(8,128)(2,1)S(1)}, bf16[2,32,2048]{2,1,0:T(8,128)(2,1)S(1)}, u32[]{:S(2)}, u32[]{:S(2)}) %collective-permute-start.5) | collective-permute-done | bytes 262176 | tf_op jit(solution)/shard_map/ppermute | solution.py:267
  142.1 2.3 %collective-permute-done.6 = bf16[2,32,2048]{2,1,0:T(8,128)(2,1)S(1)} collective-permute-done((bf16[2,32,2048]{2,1,0:T(8,128)(2,1)S(1)}, bf16[2,32,2048]{2,1,0:T(8,128)(2,1)S(1)}, u32[]{:S(2)}, u32[]{:S(2)}) %collective-permute-start.6) | collective-permute-done | bytes 262176 | tf_op jit(solution)/shard_map/ppermute | solution.py:267
  144.4 0.1 pad_maximum_fusion.mine_ref
  144.5 0.0 copy-start.4
  144.6 4.1 %collective-permute-start.7 = (bf16[4,2,32,2048]{3,2,1,0:T(8,128)(2,1)S(1)}, bf16[4,2,32,2048]{3,2,1,0:T(8,128)(2,1)S(1)}, u32[]{:S(2)}, u32[]{:S(2)}) collective-permute-start(bf16[4,2,32,2048]{3,2,1,0:T(8,128)(2,1)S(1)} %pad_maximum_fusion.mine_ref), channel_id=1, source_target_pairs={{0,1},{1,0},{2,3},{3,2},{4,5},{5,4},{6,7},{7,6},{8,9},{9,8},{10,11... | collective-permute-start | bytes 3145736 | tf_op jit(solution)/shard_map/ppermute | solution.py:263
  148.6 0.0 all-to-all-done.1
  148.7 2.7 %reduce_sum.21 = bf16[256,512]{1,0:T(8,128)(2,1)} reduce(bf16[8,256,512]{2,1,0:T(8,128)(2,1)} %all-to-all-done.1, bf16[]{:T(256)} %constant.52.clone.1), dimensions={0}, to_apply=%region_0.0 | reduce | flops 917504 | bytes 2359298 | tf_op jit(solution)/shard_map/reduce_sum | solution.py:275
  151.3 6.9 %all-to-all-start.2 = ((bf16[8,32,512]{2,1,0:T(8,128)(2,1)}), bf16[8,32,512]{2,1,0:T(8,128)(2,1)S(1)}, u32[]{:S(2)}, u32[]{:S(2)}) async-start(bf16[8,32,512]{2,1,0:T(8,128)(2,1)} %bitcast.17), calls=%async_computation.2 | async-start | bytes 524288 | tf_op jit(solution)/shard_map/all_to_all | solution.py:299
  158.2 0.1 pad_add_fusion.place_ref
  158.3 0.0 collective-permute-done.7.other_ref
  158.3 2.0 %assemble.1 = (bf16[256,2048]{1,0:T(8,128)(2,1)}, bf16[256,2048]{1,0:T(8,128)(2,1)}) custom-call(s32[2]{0:T(128)S(1)} %pad_add_fusion.place_ref, bf16[4,2,32,2048]{3,2,1,0:T(8,128)(2,1)S(1)} %pad_maximum_fusion.mine_ref, bf16[4,2,32,2048]{3,2,1,0:T(8,128)(2,1)S(1)} %collective-permute-done.7.other_ref), custom_call_target="tpu_custom_call" | custom-call | tf_op jit(solution)/shard_map/assemble/pallas_call | solution.py:251
  160.3 7.6 %all-to-all-done.2 = bf16[8,32,512]{2,1,0:T(8,128)(2,1)S(1)} async-done(((bf16[8,32,512]{2,1,0:T(8,128)(2,1)}), bf16[8,32,512]{2,1,0:T(8,128)(2,1)S(1)}, u32[]{:S(2)}, u32[]{:S(2)}) %all-to-all-start.2) | async-done | bytes 262176 | tf_op jit(solution)/shard_map/all_to_all | solution.py:299
  167.9 0.0 copy-done.4
  167.9 0.6 bitcast_add_fusion.1
  (2 shorter events, 0.0 us)
Async XLA Ops:
  7.2 28.2 %copy-start = (f32[3,4096]{1,0:T(4,128)S(1)}, f32[3,4096]{1,0:T(4,128)}, u32[]{:S(2)}) copy-start(f32[3,4096]{1,0:T(4,128)} %param.15) | copy-start | bytes 147460
  7.2 26.8 %copy-start.3 = (bf16[256,2048]{1,0:T(8,128)(2,1)S(1)}, bf16[256,2048]{1,0:T(8,128)(2,1)}, u32[]{:S(2)}) copy-start(bf16[256,2048]{1,0:T(8,128)(2,1)} %cot_hbm.1) | copy-start | bytes 3145732
  7.2 71.9 %all-gather.3.cloned.1.call-start = ((), (), s32[]{:S(2)}) async-start(), calls=%async_computation.3 | async-start | bytes 7077888 | tf_op jit(solution)/shard_map/all_gather | solution.py:289
  86.4 0.8 copy-start.1
  87.2 0.8 copy-start.2
  88.0 60.7 %all-to-all-start.1 = ((bf16[8,256,512]{2,1,0:T(8,128)(2,1)}), bf16[8,256,512]{2,1,0:T(8,128)(2,1)}, u32[]{:S(2)}, u32[]{:S(2)}) async-start(bf16[8,256,512]{2,1,0:T(8,128)(2,1)} %bitcast.16), calls=%async_computation.1 | async-start | bytes 4194304 | tf_op jit(solution)/shard_map/all_to_all | solution.py:295
  101.9 6.2 %collective-permute-start = (bf16[4,2,32,2048]{3,2,1,0:T(8,128)(2,1)S(1)}, bf16[4,2,32,2048]{3,2,1,0:T(8,128)(2,1)S(1)}, u32[]{:S(2)}, u32[]{:S(2)}) collective-permute-start(bf16[4,2,32,2048]{3,2,1,0:T(8,128)(2,1)S(1)} %get-tuple-element.13), channel_id=1, source_target_pairs={{0,1},{1,0},{2,3},{3,2},{4,5},{5,4},{6,7},{7,6},{8,9},{9,8},{10,11... | collective-permute-start | bytes 3145736 | tf_op jit(solution)/shard_map/ppermute | solution.py:263
  108.4 11.1 %collective-permute-start.1 = (bf16[2,32,2048]{2,1,0:T(8,128)(2,1)S(1)}, bf16[2,32,2048]{2,1,0:T(8,128)(2,1)S(1)}, u32[]{:S(2)}, u32[]{:S(2)}) collective-permute-start(bf16[2,32,2048]{2,1,0:T(8,128)(2,1)S(1)} %get-tuple-element.17), channel_id=1, source_target_pairs={{0,4},{2,6},{4,0},{6,2},{1,5},{3,7},{5,1},{7,3},{8,12},{10,14},{12... | collective-permute-start | bytes 786440 | tf_op jit(solution)/shard_map/ppermute | solution.py:267
  113.0 12.4 %collective-permute-start.2 = (bf16[2,32,2048]{2,1,0:T(8,128)(2,1)S(1)}, bf16[2,32,2048]{2,1,0:T(8,128)(2,1)S(1)}, u32[]{:S(2)}, u32[]{:S(2)}) collective-permute-start(bf16[2,32,2048]{2,1,0:T(8,128)(2,1)S(1)} %get-tuple-element.19), channel_id=1, source_target_pairs={{0,2},{2,4},{4,6},{6,0},{1,3},{3,5},{5,7},{7,1},{8,10},{10,12},{12... | collective-permute-start | bytes 786440 | tf_op jit(solution)/shard_map/ppermute | solution.py:267
  115.2 10.2 %collective-permute-start.3 = (bf16[2,32,2048]{2,1,0:T(8,128)(2,1)S(1)}, bf16[2,32,2048]{2,1,0:T(8,128)(2,1)}, u32[]{:S(2)}, u32[]{:S(2)}) collective-permute-start(bf16[2,32,2048]{2,1,0:T(8,128)(2,1)S(1)} %get-tuple-element.18), channel_id=1, source_target_pairs={{0,6},{2,0},{4,2},{6,4},{1,7},{3,1},{5,3},{7,5},{8,14},{10,8},{12,... | collective-permute-start | bytes 786440 | tf_op jit(solution)/shard_map/ppermute | solution.py:267
  126.5 10.8 %collective-permute-start.4 = (bf16[2,32,2048]{2,1,0:T(8,128)(2,1)S(1)}, bf16[2,32,2048]{2,1,0:T(8,128)(2,1)S(1)}, u32[]{:S(2)}, u32[]{:S(2)}) collective-permute-start(bf16[2,32,2048]{2,1,0:T(8,128)(2,1)S(1)} %fusion.2), channel_id=1, source_target_pairs={{0,2},{2,4},{4,6},{6,0},{1,3},{3,5},{5,7},{7,1},{8,10},{10,12},{12... | collective-permute-start | bytes 786440 | tf_op jit(solution)/shard_map/ppermute | solution.py:267
  129.9 12.2 %collective-permute-start.5 = (bf16[2,32,2048]{2,1,0:T(8,128)(2,1)S(1)}, bf16[2,32,2048]{2,1,0:T(8,128)(2,1)S(1)}, u32[]{:S(2)}, u32[]{:S(2)}) collective-permute-start(bf16[2,32,2048]{2,1,0:T(8,128)(2,1)S(1)} %fusion.2), channel_id=1, source_target_pairs={{0,4},{2,6},{4,0},{6,2},{1,5},{3,7},{5,1},{7,3},{8,12},{10,14},{12... | collective-permute-start | bytes 786440 | tf_op jit(solution)/shard_map/ppermute | solution.py:267
  133.8 10.6 %collective-permute-start.6 = (bf16[2,32,2048]{2,1,0:T(8,128)(2,1)S(1)}, bf16[2,32,2048]{2,1,0:T(8,128)(2,1)S(1)}, u32[]{:S(2)}, u32[]{:S(2)}) collective-permute-start(bf16[2,32,2048]{2,1,0:T(8,128)(2,1)S(1)} %fusion.2), channel_id=1, source_target_pairs={{0,6},{2,0},{4,2},{6,4},{1,7},{3,1},{5,3},{7,5},{8,14},{10,8},{12,... | collective-permute-start | bytes 786440 | tf_op jit(solution)/shard_map/ppermute | solution.py:267
  144.5 23.3 %copy-start.4 = (f32[512,32]{0,1:T(8,128)S(1)}, f32[512,32]{0,1:T(8,128)}, u32[]{:S(2)}) copy-start(f32[512,32]{0,1:T(8,128)} %param.17) | copy-start | bytes 196612
  144.6 13.7 %collective-permute-start.7 = (bf16[4,2,32,2048]{3,2,1,0:T(8,128)(2,1)S(1)}, bf16[4,2,32,2048]{3,2,1,0:T(8,128)(2,1)S(1)}, u32[]{:S(2)}, u32[]{:S(2)}) collective-permute-start(bf16[4,2,32,2048]{3,2,1,0:T(8,128)(2,1)S(1)} %pad_maximum_fusion.mine_ref), channel_id=1, source_target_pairs={{0,1},{1,0},{2,3},{3,2},{4,5},{5,4},{6,7},{7,6},{8,9},{9,8},{10,11... | collective-permute-start | bytes 3145736 | tf_op jit(solution)/shard_map/ppermute | solution.py:263
  151.3 16.5 %all-to-all-start.2 = ((bf16[8,32,512]{2,1,0:T(8,128)(2,1)}), bf16[8,32,512]{2,1,0:T(8,128)(2,1)S(1)}, u32[]{:S(2)}, u32[]{:S(2)}) async-start(bf16[8,32,512]{2,1,0:T(8,128)(2,1)} %bitcast.17), calls=%async_computation.2 | async-start | bytes 524288 | tf_op jit(solution)/shard_map/all_to_all | solution.py:299
Sparse Core Ops, SparseCore 0:
  34.0 45.0 all-gather.2

commit v2 on v1

--- a/solution.py
+++ b/solution.py
@@ -103,7 +103,8 @@
 
 def early_kernel(
     stride_ref, taps_ref, bias_ref, xe_hbm, cot_t_ref, w_hbm,
-    grad_ref, act_ref, slope_ref, w_ref, xe_ref, w_sems, x_sems,
+    grad_hbm, act_hbm, slope_hbm,
+    w_ref, xe_ref, grad_ref, act_ref, slope_ref, w_sems, x_sems, grad_sems, field_sems,
 ):
     outer = stride_ref[0]
     inner = stride_ref[1]
@@ -115,14 +116,28 @@
     act = conv * sig
     act_ref[...] = act
     slope_ref[...] = up * sig * (1.0 + conv * (1.0 - sig))
+    sent = [
+        pltpu.make_async_copy(act_ref, act_hbm, field_sems.at[0]),
+        pltpu.make_async_copy(slope_ref, slope_hbm, field_sems.at[1]),
+    ]
+    for c in sent:
+        c.start()
     hidden = (act * up).astype(jnp.bfloat16)
     for k in range(8):
-        part = jnp.dot(
+        grad_ref[k * 256 : (k + 1) * 256, :] = jnp.dot(
             cot_t_ref[k * 256 : (k + 1) * 256, :], hidden, preferred_element_type=jnp.float32
         ).astype(jnp.bfloat16)
         for j in range(8):
             at = pl.multiple_of((k * outer + j * inner) * 32, 32)
-            grad_ref[pl.ds(at, 32), :] = part[j * 32 : (j + 1) * 32, :]
+            block = pltpu.make_async_copy(
+                grad_ref.at[pl.ds((k * 8 + j) * 32, 32)],
+                grad_hbm.at[pl.ds(at, 32)],
+                grad_sems.at[k, j],
+            )
+            block.start()
+            sent.append(block)
+    for c in sent:
+        c.wait()
 
 
 def outputs_kernel(
@@ -187,12 +202,17 @@
         early_kernel,
         out_shape=(jax.ShapeDtypeStruct((WIDTH, UNITS), jnp.bfloat16), FIELD, FIELD),
         in_specs=[SMEM, VMEM, VMEM, HBM, VMEM, HBM],
-        out_specs=(VMEM, VMEM, VMEM),
+        out_specs=(HBM, HBM, HBM),
         scratch_shapes=[
             W_SPACE,
             X_SPACE,
+            pltpu.VMEM((WIDTH, UNITS), jnp.bfloat16),
+            F_SPACE,
+            F_SPACE,
             pltpu.SemaphoreType.DMA((1, 8, 8)),
             pltpu.SemaphoreType.DMA((4,)),
+            pltpu.SemaphoreType.DMA((8, 8)),
+            pltpu.SemaphoreType.DMA((2,)),
         ],
         compiler_params=pltpu.CompilerParams(vmem_limit_bytes=36 * 1024 * 1024),
         cost_estimate=pl.CostEstimate(

time: 176 us -> 177 us (level)
  no operation moved by 1% of the time
where the time goes in v2:
time: 177 us; the launch traced here: 176 us
  waiting for transfers between devices  66.6 us (38%)
  starting transfers between devices  41.1 us (23%)
  blocking collectives  25.7 us (15%)
  Pallas kernels  19 us (11%)
  between operations  14.3 us (8%)
  other arithmetic  5.89 us (3%)
  local copies, waits for them, and re-layouts  2.95 us (2%)
    all_gather x1, waiting for transfers between devices, shards(): w = lax.all_gather(near, AXES, axis_index_groups=SECOND)  43.8 us
    all_to_all x1, blocking collectives, shards(): lax.all_to_all(jnp.broadcast_to(mine[None], (8,) + mine.shape), AXES, 0,...  25.7 us
    ppermute x6, starting transfers between devices, moved(): return lax.ppermute(value, 'x', [(i, (i + steps) % NX) for i in range(NX)])  21.8 us
    ppermute x6, waiting for transfers between devices, moved(): return lax.ppermute(value, 'x', [(i, (i + steps) % NX) for i in range(NX)])  13 us
    pallas_call x1, Pallas kernels, outputs(): pl.pallas_call(outputs_kernel, out_shape=(piece, piece), in_specs=[SMEM,...  9.53 us
    ppermute x2, starting transfers between devices, exchanged(): return lax.ppermute(value, 'c', [(0, 1), (1, 0)])  8.03 us
    all_to_all x1, waiting for transfers between devices, shards(): grad = lax.all_to_all(grad, AXES, 0, 0, tiled=True, axis_index_groups=FIRST)  7.56 us
    pallas_call x1, Pallas kernels, early(): pl.pallas_call(early_kernel, out_shape=(jax.ShapeDtypeStruct((WIDTH, UNIT...  7.49 us
  transfers between devices with their start and end apart: 11, of which 6 were waited for; matrix products, arithmetic and copies ran while one was open for 3% of the time, Pallas kernels for 7%

profile of v2, /device:TPU:1, one launch (start us, length us, event | category | flops | bytes accessed | tf_op | source)
XLA Modules:
  0.0 175.6 jit_solution(337283502325601126)
XLA Ops:
  7.2 0.0 copy-start
  7.2 0.0 copy-start.3
  7.2 0.0 all-gather.3.cloned.1.call-start
  7.2 0.9 pad_maximum_fusion.1
  8.1 0.1 broadcast_in_dim.10
  8.2 25.7 %all_to_all.15 = bf16[8,32,1536]{2,1,0:T(8,128)(2,1)} all-to-all(bf16[8,32,1536]{2,1,0:T(8,128)(2,1)S(1)} %broadcast_in_dim.10), channel_id=1, replica_groups={{0,8,16,24,32,40,48,56},{1,65,129,193,257,321,385,449},{64,72,80,88,96,..., dimensions={0} | all-to-all | bytes 1572864 | tf_op jit(solution)/shard_map/all_to_all | solution.py:305
  33.9 0.0 all-gather.3.cloned.1.call-update
  33.9 0.0 copy-done.3
  33.9 0.5 copy.14
  34.5 0.8 dynamic_slice.32
  35.2 0.1 pad_add_fusion.1.stride_ref
  35.3 0.0 copy-done
  35.3 43.8 %all-gather.3.cloned.1.call-done = bf16[64,32,1536]{2,1,0:T(8,128)(2,1)} async-done(((bf16[8,32,1536]{2,1,0:T(8,128)(2,1)}), bf16[64,32,1536]{2,1,0:T(8,128)(2,1)}) %all-gather.3.cloned.1.call-update) | async-done | bytes 6291472 | tf_op jit(solution)/shard_map/all_gather | solution.py:309
  79.1 7.5 %early.1 = (bf16[2048,512]{1,0:T(8,128)(2,1)}, f32[256,512]{1,0:T(8,128)S(1)}, f32[256,512]{1,0:T(8,128)S(1)}) custom-call(s32[2]{0:T(128)S(1)} %pad_add_fusion.1.stride_ref, f32[3,512]{1,0:T(4,128)S(1)} %constant_dynamic-slice_fusion.taps_ref, f32[1,512]{1,0:T(1,128)S(1)} %bitcast.31, bf16[256,2048]{1,0:T(8,128)(2,1)} %xe_hbm.1, ...), custom_call_target="tpu_custom_call" | custom-call | flops 3000000000 | bytes 8000000 | tf_op jit(solution)/shard_map/early/pallas_call | solution.py:201
  86.6 0.0 copy-start.1
  86.6 0.8 copy-done.1
  87.4 0.0 copy-start.2
  87.4 0.8 copy-done.2
  88.2 4.4 %all-to-all-start.1 = ((bf16[8,256,512]{2,1,0:T(8,128)(2,1)}), bf16[8,256,512]{2,1,0:T(8,128)(2,1)}, u32[]{:S(2)}, u32[]{:S(2)}) async-start(bf16[8,256,512]{2,1,0:T(8,128)(2,1)} %bitcast.16), calls=%async_computation.1 | async-start | bytes 4194304 | tf_op jit(solution)/shard_map/all_to_all | solution.py:315
  92.6 9.5 %outputs.1 = (bf16[4,2,32,2048]{3,2,1,0:T(8,128)(2,1)S(1)}, bf16[4,2,32,2048]{3,2,1,0:T(8,128)(2,1)S(1)}) custom-call(s32[2]{0:T(128)S(1)} %pad_add_fusion.1.stride_ref, f32[3,512]{1,0:T(4,128)S(1)} %constant_dynamic-slice_fusion.taps_ref, f32[1,512]{1,0:T(1,128)S(1)} %bitcast.32, bf16[256,2048]{1,0:T(8,128)(2,1)} %xl_hbm.1, bf16[256,2048]{1,0:T(8,128)(2,1)} %cot_hbm.1, ...), custom_call_target="tpu_custom_call" | custom-call | flops 4000000000 | bytes 12000000 | tf_op jit(solution)/shard_map/outputs/pallas_call | solution.py:227
  102.1 3.9 %collective-permute-start = (bf16[4,2,32,2048]{3,2,1,0:T(8,128)(2,1)S(1)}, bf16[4,2,32,2048]{3,2,1,0:T(8,128)(2,1)S(1)}, u32[]{:S(2)}, u32[]{:S(2)}) collective-permute-start(bf16[4,2,32,2048]{3,2,1,0:T(8,128)(2,1)S(1)} %get-tuple-element.13), channel_id=1, source_target_pairs={{0,1},{1,0},{2,3},{3,2},{4,5},{5,4},{6,7},{7,6},{8,9},{9,8},{10,11... | collective-permute-start | bytes 3145736 | tf_op jit(solution)/shard_map/ppermute | solution.py:283
  106.1 2.2 %collective-permute-done = bf16[4,2,32,2048]{3,2,1,0:T(8,128)(2,1)S(1)} collective-permute-done((bf16[4,2,32,2048]{3,2,1,0:T(8,128)(2,1)S(1)}, bf16[4,2,32,2048]{3,2,1,0:T(8,128)(2,1)S(1)}, u32[]{:S(2)}, u32[]{:S(2)}) %collective-permute-start) | collective-permute-done | bytes 1048608 | tf_op jit(solution)/shard_map/ppermute | solution.py:283
  108.3 0.3 fusion.3
  108.6 4.6 %collective-permute-start.1 = (bf16[2,32,2048]{2,1,0:T(8,128)(2,1)S(1)}, bf16[2,32,2048]{2,1,0:T(8,128)(2,1)S(1)}, u32[]{:S(2)}, u32[]{:S(2)}) collective-permute-start(bf16[2,32,2048]{2,1,0:T(8,128)(2,1)S(1)} %get-tuple-element.17), channel_id=1, source_target_pairs={{0,4},{2,6},{4,0},{6,2},{1,5},{3,7},{5,1},{7,3},{8,12},{10,14},{12... | collective-permute-start | bytes 786440 | tf_op jit(solution)/shard_map/ppermute | solution.py:287
  113.2 2.2 %collective-permute-start.2 = (bf16[2,32,2048]{2,1,0:T(8,128)(2,1)S(1)}, bf16[2,32,2048]{2,1,0:T(8,128)(2,1)S(1)}, u32[]{:S(2)}, u32[]{:S(2)}) collective-permute-start(bf16[2,32,2048]{2,1,0:T(8,128)(2,1)S(1)} %get-tuple-element.19), channel_id=1, source_target_pairs={{0,2},{2,4},{4,6},{6,0},{1,3},{3,5},{5,7},{7,1},{8,10},{10,12},{12... | collective-permute-start | bytes 786440 | tf_op jit(solution)/shard_map/ppermute | solution.py:287
  115.4 4.3 %collective-permute-start.3 = (bf16[2,32,2048]{2,1,0:T(8,128)(2,1)S(1)}, bf16[2,32,2048]{2,1,0:T(8,128)(2,1)}, u32[]{:S(2)}, u32[]{:S(2)}) collective-permute-start(bf16[2,32,2048]{2,1,0:T(8,128)(2,1)S(1)} %get-tuple-element.18), channel_id=1, source_target_pairs={{0,6},{2,0},{4,2},{6,4},{1,7},{3,1},{5,3},{7,5},{8,14},{10,8},{12,... | collective-permute-start | bytes 786440 | tf_op jit(solution)/shard_map/ppermute | solution.py:287
  119.7 0.0 collective-permute-done.1
  119.7 5.9 %collective-permute-done.2 = bf16[2,32,2048]{2,1,0:T(8,128)(2,1)S(1)} collective-permute-done((bf16[2,32,2048]{2,1,0:T(8,128)(2,1)S(1)}, bf16[2,32,2048]{2,1,0:T(8,128)(2,1)S(1)}, u32[]{:S(2)}, u32[]{:S(2)}) %collective-permute-start.2) | collective-permute-done | bytes 262176 | tf_op jit(solution)/shard_map/ppermute | solution.py:287
  125.6 0.0 collective-permute-done.3
  125.6 1.1 fusion.2
  126.7 3.4 %collective-permute-start.4 = (bf16[2,32,2048]{2,1,0:T(8,128)(2,1)S(1)}, bf16[2,32,2048]{2,1,0:T(8,128)(2,1)S(1)}, u32[]{:S(2)}, u32[]{:S(2)}) collective-permute-start(bf16[2,32,2048]{2,1,0:T(8,128)(2,1)S(1)} %fusion.2), channel_id=1, source_target_pairs={{0,2},{2,4},{4,6},{6,0},{1,3},{3,5},{5,7},{7,1},{8,10},{10,12},{12... | collective-permute-start | bytes 786440 | tf_op jit(solution)/shard_map/ppermute | solution.py:287
  130.1 3.9 %collective-permute-start.5 = (bf16[2,32,2048]{2,1,0:T(8,128)(2,1)S(1)}, bf16[2,32,2048]{2,1,0:T(8,128)(2,1)S(1)}, u32[]{:S(2)}, u32[]{:S(2)}) collective-permute-start(bf16[2,32,2048]{2,1,0:T(8,128)(2,1)S(1)} %fusion.2), channel_id=1, source_target_pairs={{0,4},{2,6},{4,0},{6,2},{1,5},{3,7},{5,1},{7,3},{8,12},{10,14},{12... | collective-permute-start | bytes 786440 | tf_op jit(solution)/shard_map/ppermute | solution.py:287
  134.0 3.4 %collective-permute-start.6 = (bf16[2,32,2048]{2,1,0:T(8,128)(2,1)S(1)}, bf16[2,32,2048]{2,1,0:T(8,128)(2,1)S(1)}, u32[]{:S(2)}, u32[]{:S(2)}) collective-permute-start(bf16[2,32,2048]{2,1,0:T(8,128)(2,1)S(1)} %fusion.2), channel_id=1, source_target_pairs={{0,6},{2,0},{4,2},{6,4},{1,7},{3,1},{5,3},{7,5},{8,14},{10,8},{12,... | collective-permute-start | bytes 786440 | tf_op jit(solution)/shard_map/ppermute | solution.py:287
  137.5 0.0 collective-permute-done.4
  137.5 4.9 %collective-permute-done.5 = bf16[2,32,2048]{2,1,0:T(8,128)(2,1)S(1)} collective-permute-done((bf16[2,32,2048]{2,1,0:T(8,128)(2,1)S(1)}, bf16[2,32,2048]{2,1,0:T(8,128)(2,1)S(1)}, u32[]{:S(2)}, u32[]{:S(2)}) %collective-permute-start.5) | collective-permute-done | bytes 262176 | tf_op jit(solution)/shard_map/ppermute | solution.py:287
  142.3 2.3 %collective-permute-done.6 = bf16[2,32,2048]{2,1,0:T(8,128)(2,1)S(1)} collective-permute-done((bf16[2,32,2048]{2,1,0:T(8,128)(2,1)S(1)}, bf16[2,32,2048]{2,1,0:T(8,128)(2,1)S(1)}, u32[]{:S(2)}, u32[]{:S(2)}) %collective-permute-start.6) | collective-permute-done | bytes 262176 | tf_op jit(solution)/shard_map/ppermute | solution.py:287
  144.6 0.1 pad_maximum_fusion.mine_ref
  144.7 0.0 copy-start.4
  144.8 4.1 %collective-permute-start.7 = (bf16[4,2,32,2048]{3,2,1,0:T(8,128)(2,1)S(1)}, bf16[4,2,32,2048]{3,2,1,0:T(8,128)(2,1)S(1)}, u32[]{:S(2)}, u32[]{:S(2)}) collective-permute-start(bf16[4,2,32,2048]{3,2,1,0:T(8,128)(2,1)S(1)} %pad_maximum_fusion.mine_ref), channel_id=1, source_target_pairs={{0,1},{1,0},{2,3},{3,2},{4,5},{5,4},{6,7},{7,6},{8,9},{9,8},{10,11... | collective-permute-start | bytes 3145736 | tf_op jit(solution)/shard_map/ppermute | solution.py:283
  148.9 0.0 all-to-all-done.1
  148.9 2.7 %reduce_sum.21 = bf16[256,512]{1,0:T(8,128)(2,1)} reduce(bf16[8,256,512]{2,1,0:T(8,128)(2,1)} %all-to-all-done.1, bf16[]{:T(256)} %constant.52.clone.1), dimensions={0}, to_apply=%region_0.0 | reduce | flops 917504 | bytes 2359298 | tf_op jit(solution)/shard_map/reduce_sum | solution.py:295
  151.5 6.9 %all-to-all-start.2 = ((bf16[8,32,512]{2,1,0:T(8,128)(2,1)}), bf16[8,32,512]{2,1,0:T(8,128)(2,1)S(1)}, u32[]{:S(2)}, u32[]{:S(2)}) async-start(bf16[8,32,512]{2,1,0:T(8,128)(2,1)} %bitcast.17), calls=%async_computation.2 | async-start | bytes 524288 | tf_op jit(solution)/shard_map/all_to_all | solution.py:319
  158.4 0.1 pad_add_fusion.place_ref
  158.5 0.0 collective-permute-done.7.other_ref
  158.5 2.0 %assemble.1 = (bf16[256,2048]{1,0:T(8,128)(2,1)}, bf16[256,2048]{1,0:T(8,128)(2,1)}) custom-call(s32[2]{0:T(128)S(1)} %pad_add_fusion.place_ref, bf16[4,2,32,2048]{3,2,1,0:T(8,128)(2,1)S(1)} %pad_maximum_fusion.mine_ref, bf16[4,2,32,2048]{3,2,1,0:T(8,128)(2,1)S(1)} %collective-permute-done.7.other_ref), custom_call_target="tpu_custom_call" | custom-call | tf_op jit(solution)/shard_map/assemble/pallas_call | solution.py:271
  160.5 7.6 %all-to-all-done.2 = bf16[8,32,512]{2,1,0:T(8,128)(2,1)S(1)} async-done(((bf16[8,32,512]{2,1,0:T(8,128)(2,1)}), bf16[8,32,512]{2,1,0:T(8,128)(2,1)S(1)}, u32[]{:S(2)}, u32[]{:S(2)}) %all-to-all-start.2) | async-done | bytes 262176 | tf_op jit(solution)/shard_map/all_to_all | solution.py:319
  168.1 0.0 copy-done.4
  168.1 0.6 bitcast_add_fusion.1
  (2 shorter events, 0.0 us)
Async XLA Ops:
  7.2 28.2 %copy-start = (f32[3,4096]{1,0:T(4,128)S(1)}, f32[3,4096]{1,0:T(4,128)}, u32[]{:S(2)}) copy-start(f32[3,4096]{1,0:T(4,128)} %param.15) | copy-start | bytes 147460
  7.2 26.8 %copy-start.3 = (bf16[256,2048]{1,0:T(8,128)(2,1)S(1)}, bf16[256,2048]{1,0:T(8,128)(2,1)}, u32[]{:S(2)}) copy-start(bf16[256,2048]{1,0:T(8,128)(2,1)} %cot_hbm.1) | copy-start | bytes 3145732
  7.2 71.9 %all-gather.3.cloned.1.call-start = ((), (), s32[]{:S(2)}) async-start(), calls=%async_computation.3 | async-start | bytes 7077888 | tf_op jit(solution)/shard_map/all_gather | solution.py:309
  86.6 0.8 copy-start.1
  87.4 0.8 copy-start.2
  88.2 60.7 %all-to-all-start.1 = ((bf16[8,256,512]{2,1,0:T(8,128)(2,1)}), bf16[8,256,512]{2,1,0:T(8,128)(2,1)}, u32[]{:S(2)}, u32[]{:S(2)}) async-start(bf16[8,256,512]{2,1,0:T(8,128)(2,1)} %bitcast.16), calls=%async_computation.1 | async-start | bytes 4194304 | tf_op jit(solution)/shard_map/all_to_all | solution.py:315
  102.1 6.2 %collective-permute-start = (bf16[4,2,32,2048]{3,2,1,0:T(8,128)(2,1)S(1)}, bf16[4,2,32,2048]{3,2,1,0:T(8,128)(2,1)S(1)}, u32[]{:S(2)}, u32[]{:S(2)}) collective-permute-start(bf16[4,2,32,2048]{3,2,1,0:T(8,128)(2,1)S(1)} %get-tuple-element.13), channel_id=1, source_target_pairs={{0,1},{1,0},{2,3},{3,2},{4,5},{5,4},{6,7},{7,6},{8,9},{9,8},{10,11... | collective-permute-start | bytes 3145736 | tf_op jit(solution)/shard_map/ppermute | solution.py:283
  108.6 11.1 %collective-permute-start.1 = (bf16[2,32,2048]{2,1,0:T(8,128)(2,1)S(1)}, bf16[2,32,2048]{2,1,0:T(8,128)(2,1)S(1)}, u32[]{:S(2)}, u32[]{:S(2)}) collective-permute-start(bf16[2,32,2048]{2,1,0:T(8,128)(2,1)S(1)} %get-tuple-element.17), channel_id=1, source_target_pairs={{0,4},{2,6},{4,0},{6,2},{1,5},{3,7},{5,1},{7,3},{8,12},{10,14},{12... | collective-permute-start | bytes 786440 | tf_op jit(solution)/shard_map/ppermute | solution.py:287
  113.2 12.4 %collective-permute-start.2 = (bf16[2,32,2048]{2,1,0:T(8,128)(2,1)S(1)}, bf16[2,32,2048]{2,1,0:T(8,128)(2,1)S(1)}, u32[]{:S(2)}, u32[]{:S(2)}) collective-permute-start(bf16[2,32,2048]{2,1,0:T(8,128)(2,1)S(1)} %get-tuple-element.19), channel_id=1, source_target_pairs={{0,2},{2,4},{4,6},{6,0},{1,3},{3,5},{5,7},{7,1},{8,10},{10,12},{12... | collective-permute-start | bytes 786440 | tf_op jit(solution)/shard_map/ppermute | solution.py:287
  115.4 10.2 %collective-permute-start.3 = (bf16[2,32,2048]{2,1,0:T(8,128)(2,1)S(1)}, bf16[2,32,2048]{2,1,0:T(8,128)(2,1)}, u32[]{:S(2)}, u32[]{:S(2)}) collective-permute-start(bf16[2,32,2048]{2,1,0:T(8,128)(2,1)S(1)} %get-tuple-element.18), channel_id=1, source_target_pairs={{0,6},{2,0},{4,2},{6,4},{1,7},{3,1},{5,3},{7,5},{8,14},{10,8},{12,... | collective-permute-start | bytes 786440 | tf_op jit(solution)/shard_map/ppermute | solution.py:287
  126.7 10.7 %collective-permute-start.4 = (bf16[2,32,2048]{2,1,0:T(8,128)(2,1)S(1)}, bf16[2,32,2048]{2,1,0:T(8,128)(2,1)S(1)}, u32[]{:S(2)}, u32[]{:S(2)}) collective-permute-start(bf16[2,32,2048]{2,1,0:T(8,128)(2,1)S(1)} %fusion.2), channel_id=1, source_target_pairs={{0,2},{2,4},{4,6},{6,0},{1,3},{3,5},{5,7},{7,1},{8,10},{10,12},{12... | collective-permute-start | bytes 786440 | tf_op jit(solution)/shard_map/ppermute | solution.py:287
  130.1 12.2 %collective-permute-start.5 = (bf16[2,32,2048]{2,1,0:T(8,128)(2,1)S(1)}, bf16[2,32,2048]{2,1,0:T(8,128)(2,1)S(1)}, u32[]{:S(2)}, u32[]{:S(2)}) collective-permute-start(bf16[2,32,2048]{2,1,0:T(8,128)(2,1)S(1)} %fusion.2), channel_id=1, source_target_pairs={{0,4},{2,6},{4,0},{6,2},{1,5},{3,7},{5,1},{7,3},{8,12},{10,14},{12... | collective-permute-start | bytes 786440 | tf_op jit(solution)/shard_map/ppermute | solution.py:287
  134.0 10.6 %collective-permute-start.6 = (bf16[2,32,2048]{2,1,0:T(8,128)(2,1)S(1)}, bf16[2,32,2048]{2,1,0:T(8,128)(2,1)S(1)}, u32[]{:S(2)}, u32[]{:S(2)}) collective-permute-start(bf16[2,32,2048]{2,1,0:T(8,128)(2,1)S(1)} %fusion.2), channel_id=1, source_target_pairs={{0,6},{2,0},{4,2},{6,4},{1,7},{3,1},{5,3},{7,5},{8,14},{10,8},{12,... | collective-permute-start | bytes 786440 | tf_op jit(solution)/shard_map/ppermute | solution.py:287
  144.7 23.3 %copy-start.4 = (f32[512,32]{0,1:T(8,128)S(1)}, f32[512,32]{0,1:T(8,128)}, u32[]{:S(2)}) copy-start(f32[512,32]{0,1:T(8,128)} %param.17) | copy-start | bytes 196612
  144.8 13.7 %collective-permute-start.7 = (bf16[4,2,32,2048]{3,2,1,0:T(8,128)(2,1)S(1)}, bf16[4,2,32,2048]{3,2,1,0:T(8,128)(2,1)S(1)}, u32[]{:S(2)}, u32[]{:S(2)}) collective-permute-start(bf16[4,2,32,2048]{3,2,1,0:T(8,128)(2,1)S(1)} %pad_maximum_fusion.mine_ref), channel_id=1, source_target_pairs={{0,1},{1,0},{2,3},{3,2},{4,5},{5,4},{6,7},{7,6},{8,9},{9,8},{10,11... | collective-permute-start | bytes 3145736 | tf_op jit(solution)/shard_map/ppermute | solution.py:283
  151.5 16.5 %all-to-all-start.2 = ((bf16[8,32,512]{2,1,0:T(8,128)(2,1)}), bf16[8,32,512]{2,1,0:T(8,128)(2,1)S(1)}, u32[]{:S(2)}, u32[]{:S(2)}) async-start(bf16[8,32,512]{2,1,0:T(8,128)(2,1)} %bitcast.17), calls=%async_computation.2 | async-start | bytes 524288 | tf_op jit(solution)/shard_map/all_to_all | solution.py:319
Sparse Core Ops, SparseCore 0:
  34.0 45.0 all-gather.2

commit v3 on v2

--- a/solution.py
+++ b/solution.py
@@ -102,14 +102,16 @@
 
 
 def early_kernel(
-    stride_ref, taps_ref, bias_ref, xe_hbm, cot_t_ref, w_hbm,
+    stride_ref, taps_ref, bias_ref, xe_hbm, cot_t_hbm, w_hbm,
     grad_hbm, act_hbm, slope_hbm,
-    w_ref, xe_ref, grad_ref, act_ref, slope_ref, w_sems, x_sems, grad_sems, field_sems,
+    w_ref, xe_ref, cot_t_ref, grad_ref, act_ref, slope_ref, w_sems, x_sems, grad_sems, field_sems,
 ):
     outer = stride_ref[0]
     inner = stride_ref[1]
     w_copy, x_copy = block_copies(outer == 8, w_hbm, w_ref, w_sems, xe_hbm, xe_ref, x_sems)
     start_inward(w_copy, x_copy)
+    cot_copy = pltpu.make_async_copy(cot_t_hbm, cot_t_ref, field_sems.at[2])
+    cot_copy.start()
     both = gate_and_up(w_copy, x_copy, w_ref, xe_ref)
     conv, up = conv_and_up(both, taps_ref, bias_ref)
     sig = sigmoid(conv)
@@ -123,6 +125,7 @@
     for c in sent:
         c.start()
     hidden = (act * up).astype(jnp.bfloat16)
+    cot_copy.wait()
     for k in range(8):
         grad_ref[k * 256 : (k + 1) * 256, :] = jnp.dot(
             cot_t_ref[k * 256 : (k + 1) * 256, :], hidden, preferred_element_type=jnp.float32
@@ -201,20 +204,21 @@
     return pl.pallas_call(
         early_kernel,
         out_shape=(jax.ShapeDtypeStruct((WIDTH, UNITS), jnp.bfloat16), FIELD, FIELD),
-        in_specs=[SMEM, VMEM, VMEM, HBM, VMEM, HBM],
+        in_specs=[SMEM, VMEM, VMEM, HBM, HBM, HBM],
         out_specs=(HBM, HBM, HBM),
         scratch_shapes=[
             W_SPACE,
             X_SPACE,
+            pltpu.VMEM((WIDTH, TOK), jnp.bfloat16),
             pltpu.VMEM((WIDTH, UNITS), jnp.bfloat16),
             F_SPACE,
             F_SPACE,
             pltpu.SemaphoreType.DMA((1, 8, 8)),
             pltpu.SemaphoreType.DMA((4,)),
             pltpu.SemaphoreType.DMA((8, 8)),
-            pltpu.SemaphoreType.DMA((2,)),
+            pltpu.SemaphoreType.DMA((3,)),
         ],
-        compiler_params=pltpu.CompilerParams(vmem_limit_bytes=36 * 1024 * 1024),
+        compiler_params=pltpu.CompilerParams(vmem_limit_bytes=58 * 1024 * 1024),
         cost_estimate=pl.CostEstimate(
             flops=3_000_000_000, transcendentals=0, bytes_accessed=8_000_000
         ),
@@ -327,12 +331,12 @@
         return left.astype(jnp.float32) + right.astype(jnp.float32)
 
     total = chip_piece(x)
-    for d in (2, 1, 3):
+    for d in range(1, NX):
         sent = chip_piece(lax.rem(x + d, NX)).astype(jnp.bfloat16)
         arrived = moved(sent, d)
         total = total + arrived.astype(jnp.float32)
     total = total.astype(jnp.bfloat16)
-    spread = {d: moved(total, d) for d in (2, 1, 3)}
+    spread = {d: moved(total, d) for d in range(1, NX)}
     mine = jnp.stack([total] + [spread[d] for d in range(1, NX)])
     other = exchanged(mine)
     where = jnp.stack([x, core]).astype(jnp.int32)

time: 177 us -> 177 us (level)
    all_gather x1, waiting for transfers between devices: 43.8 us -> 41.2 us  [shards(): w = lax.all_gather(near, AXES, axis_index_groups=SECOND)]
    ppermute x6, waiting for transfers between devices: 13 us -> 15.2 us  [moved(): return lax.ppermute(value, 'x', [(i, (i + steps) % NX) for i in range(NX)])]
  transfers between devices with their start and end apart: 11 -> 11, of which waited for: 6 -> 8; matrix products, arithmetic and copies ran while one was open for 3% -> 5% of each run, Pallas kernels for 7% -> 7%
where the time goes in v3:
time: 177 us; the launch traced here: 176 us
  waiting for transfers between devices  66.2 us (37%)
  starting transfers between devices  41 us (23%)
  blocking collectives  25.7 us (15%)
  Pallas kernels  19.1 us (11%)
  between operations  14.3 us (8%)
  other arithmetic  6.44 us (4%)
  local copies, waits for them, and re-layouts  3.35 us (2%)
    all_gather x1, waiting for transfers between devices, shards(): w = lax.all_gather(near, AXES, axis_index_groups=SECOND)  41.2 us
    all_to_all x1, blocking collectives, shards(): lax.all_to_all(jnp.broadcast_to(mine[None], (8,) + mine.shape), AXES, 0,...  25.7 us
    ppermute x6, starting transfers between devices, moved(): return lax.ppermute(value, 'x', [(i, (i + steps) % NX) for i in range(NX)])  21.7 us
    ppermute x6, waiting for transfers between devices, moved(): return lax.ppermute(value, 'x', [(i, (i + steps) % NX) for i in range(NX)])  15.2 us
    pallas_call x1, Pallas kernels, outputs(): pl.pallas_call(outputs_kernel, out_shape=(piece, piece), in_specs=[SMEM,...  9.53 us
    ppermute x2, starting transfers between devices, exchanged(): return lax.ppermute(value, 'c', [(0, 1), (1, 0)])  8.03 us
    pallas_call x1, Pallas kernels, early(): pl.pallas_call(early_kernel, out_shape=(jax.ShapeDtypeStruct((WIDTH, UNIT...  7.59 us
    all_to_all x1, waiting for transfers between devices, shards(): grad = lax.all_to_all(grad, AXES, 0, 0, tiled=True, axis_index_groups=FIRST)  7.56 us
  transfers between devices with their start and end apart: 11, of which 8 were waited for; matrix products, arithmetic and copies ran while one was open for 5% of the time, Pallas kernels for 7%

profile of v3, /device:TPU:1, one launch (start us, length us, event | category | flops | bytes accessed | tf_op | source)
XLA Modules:
  0.0 176.2 jit_solution(4362291495865369002)
XLA Ops:
  7.2 0.0 copy-start
  7.2 0.0 copy-start.4
  7.2 0.0 all-gather.3.cloned.1.call-start
  7.2 0.9 pad_maximum_fusion.1
  8.1 0.1 broadcast_in_dim.10
  8.2 25.7 %all_to_all.15 = bf16[8,32,1536]{2,1,0:T(8,128)(2,1)} all-to-all(bf16[8,32,1536]{2,1,0:T(8,128)(2,1)S(1)} %broadcast_in_dim.10), channel_id=1, replica_groups={{0,8,16,24,32,40,48,56},{1,65,129,193,257,321,385,449},{64,72,80,88,96,..., dimensions={0} | all-to-all | bytes 1572864 | tf_op jit(solution)/shard_map/all_to_all | solution.py:309
  33.9 0.0 all-gather.3.cloned.1.call-update
  33.9 0.0 copy-done.4
  33.9 1.3 copy.14
  35.3 1.3 dynamic_slice.32
  36.6 0.6 pad_add_fusion.1.stride_ref
  37.2 0.0 copy-done
  37.2 0.6 constant_dynamic-slice_fusion.taps_ref
  37.8 41.2 %all-gather.3.cloned.1.call-done = bf16[64,32,1536]{2,1,0:T(8,128)(2,1)} async-done(((bf16[8,32,1536]{2,1,0:T(8,128)(2,1)}), bf16[64,32,1536]{2,1,0:T(8,128)(2,1)}) %all-gather.3.cloned.1.call-update) | async-done | bytes 6291472 | tf_op jit(solution)/shard_map/all_gather | solution.py:313
  79.1 7.6 %early.1 = (bf16[2048,512]{1,0:T(8,128)(2,1)}, f32[256,512]{1,0:T(8,128)}, f32[256,512]{1,0:T(8,128)}) custom-call(s32[2]{0:T(128)} %pad_add_fusion.1.stride_ref, f32[3,512]{1,0:T(4,128)} %constant_dynamic-slice_fusion.taps_ref, f32[1,512]{1,0:T(1,128)} %bitcast.30, bf16[256,2048]{1,0:T(8,128)(2,1)} %xe_hbm.1, bf16[2048,256]{1,0:T(8,128)(2,1)} %bitcast.33, ...), custom_call_target="tpu_custom_call" | custom-call | flops 3000000000 | bytes 8000000 | tf_op jit(solution)/shard_map/early/pallas_call | solution.py:204
  86.7 0.0 copy-start.1
  86.7 0.0 copy-start.2
  86.7 0.0 copy-start.3
  86.7 4.4 %all-to-all-start.1 = ((bf16[8,256,512]{2,1,0:T(8,128)(2,1)}), bf16[8,256,512]{2,1,0:T(8,128)(2,1)}, u32[]{:S(2)}, u32[]{:S(2)}) async-start(bf16[8,256,512]{2,1,0:T(8,128)(2,1)} %bitcast.32), calls=%async_computation.1 | async-start | bytes 4194304 | tf_op jit(solution)/shard_map/all_to_all | solution.py:319
  91.1 0.0 copy-done.1
  91.1 0.0 copy-done.2
  91.1 0.0 copy-done.3
  91.1 9.5 %outputs.1 = (bf16[4,2,32,2048]{3,2,1,0:T(8,128)(2,1)S(1)}, bf16[4,2,32,2048]{3,2,1,0:T(8,128)(2,1)S(1)}) custom-call(s32[2]{0:T(128)S(1)} %copy-done.3, f32[3,512]{1,0:T(4,128)S(1)} %copy-done.1, f32[1,512]{1,0:T(1,128)S(1)} %bitcast.31, bf16[256,2048]{1,0:T(8,128)(2,1)} %xl_hbm.1, bf16[256,2048]{1,0:T(8,128)(2,1)} %cot_hbm.1, ...), custom_call_target="tpu_custom_call" | custom-call | flops 4000000000 | bytes 12000000 | tf_op jit(solution)/shard_map/outputs/pallas_call | solution.py:231
  100.7 3.9 %collective-permute-start = (bf16[4,2,32,2048]{3,2,1,0:T(8,128)(2,1)S(1)}, bf16[4,2,32,2048]{3,2,1,0:T(8,128)(2,1)S(1)}, u32[]{:S(2)}, u32[]{:S(2)}) collective-permute-start(bf16[4,2,32,2048]{3,2,1,0:T(8,128)(2,1)S(1)} %get-tuple-element.13), channel_id=1, source_target_pairs={{0,1},{1,0},{2,3},{3,2},{4,5},{5,4},{6,7},{7,6},{8,9},{9,8},{10,11... | collective-permute-start | bytes 3145736 | tf_op jit(solution)/shard_map/ppermute | solution.py:287
  104.7 2.2 %collective-permute-done = bf16[4,2,32,2048]{3,2,1,0:T(8,128)(2,1)S(1)} collective-permute-done((bf16[4,2,32,2048]{3,2,1,0:T(8,128)(2,1)S(1)}, bf16[4,2,32,2048]{3,2,1,0:T(8,128)(2,1)S(1)}, u32[]{:S(2)}, u32[]{:S(2)}) %collective-permute-start) | collective-permute-done | bytes 1048608 | tf_op jit(solution)/shard_map/ppermute | solution.py:287
  106.9 0.3 fusion.3
  107.2 3.1 %collective-permute-start.1 = (bf16[2,32,2048]{2,1,0:T(8,128)(2,1)S(1)}, bf16[2,32,2048]{2,1,0:T(8,128)(2,1)S(1)}, u32[]{:S(2)}, u32[]{:S(2)}) collective-permute-start(bf16[2,32,2048]{2,1,0:T(8,128)(2,1)S(1)} %get-tuple-element.17), channel_id=1, source_target_pairs={{0,2},{2,4},{4,6},{6,0},{1,3},{3,5},{5,7},{7,1},{8,10},{10,12},{12... | collective-permute-start | bytes 786440 | tf_op jit(solution)/shard_map/ppermute | solution.py:291
  110.3 4.3 %collective-permute-start.2 = (bf16[2,32,2048]{2,1,0:T(8,128)(2,1)S(1)}, bf16[2,32,2048]{2,1,0:T(8,128)(2,1)S(1)}, u32[]{:S(2)}, u32[]{:S(2)}) collective-permute-start(bf16[2,32,2048]{2,1,0:T(8,128)(2,1)S(1)} %get-tuple-element.19), channel_id=1, source_target_pairs={{0,4},{2,6},{4,0},{6,2},{1,5},{3,7},{5,1},{7,3},{8,12},{10,14},{12... | collective-permute-start | bytes 786440 | tf_op jit(solution)/shard_map/ppermute | solution.py:291
  114.6 3.1 %collective-permute-start.3 = (bf16[2,32,2048]{2,1,0:T(8,128)(2,1)S(1)}, bf16[2,32,2048]{2,1,0:T(8,128)(2,1)}, u32[]{:S(2)}, u32[]{:S(2)}) collective-permute-start(bf16[2,32,2048]{2,1,0:T(8,128)(2,1)S(1)} %get-tuple-element.18), channel_id=1, source_target_pairs={{0,6},{2,0},{4,2},{6,4},{1,7},{3,1},{5,3},{7,5},{8,14},{10,8},{12,... | collective-permute-start | bytes 786440 | tf_op jit(solution)/shard_map/ppermute | solution.py:291
  117.7 0.2 collective-permute-done.1
  117.9 6.4 %collective-permute-done.2 = bf16[2,32,2048]{2,1,0:T(8,128)(2,1)S(1)} collective-permute-done((bf16[2,32,2048]{2,1,0:T(8,128)(2,1)S(1)}, bf16[2,32,2048]{2,1,0:T(8,128)(2,1)S(1)}, u32[]{:S(2)}, u32[]{:S(2)}) %collective-permute-start.2) | collective-permute-done | bytes 262176 | tf_op jit(solution)/shard_map/ppermute | solution.py:291
  124.3 1.4 collective-permute-done.3
  125.7 1.1 fusion.2
  126.8 5.0 %collective-permute-start.4 = (bf16[2,32,2048]{2,1,0:T(8,128)(2,1)S(1)}, bf16[2,32,2048]{2,1,0:T(8,128)(2,1)S(1)}, u32[]{:S(2)}, u32[]{:S(2)}) collective-permute-start(bf16[2,32,2048]{2,1,0:T(8,128)(2,1)S(1)} %fusion.2), channel_id=1, source_target_pairs={{0,2},{2,4},{4,6},{6,0},{1,3},{3,5},{5,7},{7,1},{8,10},{10,12},{12... | collective-permute-start | bytes 786440 | tf_op jit(solution)/shard_map/ppermute | solution.py:291
  131.8 3.2 %collective-permute-start.5 = (bf16[2,32,2048]{2,1,0:T(8,128)(2,1)S(1)}, bf16[2,32,2048]{2,1,0:T(8,128)(2,1)S(1)}, u32[]{:S(2)}, u32[]{:S(2)}) collective-permute-start(bf16[2,32,2048]{2,1,0:T(8,128)(2,1)S(1)} %fusion.2), channel_id=1, source_target_pairs={{0,4},{2,6},{4,0},{6,2},{1,5},{3,7},{5,1},{7,3},{8,12},{10,14},{12... | collective-permute-start | bytes 786440 | tf_op jit(solution)/shard_map/ppermute | solution.py:291
  135.0 3.0 %collective-permute-start.6 = (bf16[2,32,2048]{2,1,0:T(8,128)(2,1)S(1)}, bf16[2,32,2048]{2,1,0:T(8,128)(2,1)S(1)}, u32[]{:S(2)}, u32[]{:S(2)}) collective-permute-start(bf16[2,32,2048]{2,1,0:T(8,128)(2,1)S(1)} %fusion.2), channel_id=1, source_target_pairs={{0,6},{2,0},{4,2},{6,4},{1,7},{3,1},{5,3},{7,5},{8,14},{10,8},{12,... | collective-permute-start | bytes 786440 | tf_op jit(solution)/shard_map/ppermute | solution.py:291
  138.1 0.0 collective-permute-done.4
  138.1 6.3 %collective-permute-done.5 = bf16[2,32,2048]{2,1,0:T(8,128)(2,1)S(1)} collective-permute-done((bf16[2,32,2048]{2,1,0:T(8,128)(2,1)S(1)}, bf16[2,32,2048]{2,1,0:T(8,128)(2,1)S(1)}, u32[]{:S(2)}, u32[]{:S(2)}) %collective-permute-start.5) | collective-permute-done | bytes 262176 | tf_op jit(solution)/shard_map/ppermute | solution.py:291
  144.4 0.8 collective-permute-done.6
  145.2 0.1 pad_maximum_fusion.mine_ref
  145.4 0.0 copy-start.5
  145.4 4.1 %collective-permute-start.7 = (bf16[4,2,32,2048]{3,2,1,0:T(8,128)(2,1)S(1)}, bf16[4,2,32,2048]{3,2,1,0:T(8,128)(2,1)S(1)}, u32[]{:S(2)}, u32[]{:S(2)}) collective-permute-start(bf16[4,2,32,2048]{3,2,1,0:T(8,128)(2,1)S(1)} %pad_maximum_fusion.mine_ref), channel_id=1, source_target_pairs={{0,1},{1,0},{2,3},{3,2},{4,5},{5,4},{6,7},{7,6},{8,9},{9,8},{10,11... | collective-permute-start | bytes 3145736 | tf_op jit(solution)/shard_map/ppermute | solution.py:287
  149.5 0.0 all-to-all-done.1
  149.5 2.6 %reduce_sum.21 = bf16[256,512]{1,0:T(8,128)(2,1)} reduce(bf16[8,256,512]{2,1,0:T(8,128)(2,1)} %all-to-all-done.1, bf16[]{:T(256)} %constant.52.clone.1), dimensions={0}, to_apply=%region_0.0 | reduce | flops 917504 | bytes 2359298 | tf_op jit(solution)/shard_map/reduce_sum | solution.py:299
  152.1 6.9 %all-to-all-start.2 = ((bf16[8,32,512]{2,1,0:T(8,128)(2,1)}), bf16[8,32,512]{2,1,0:T(8,128)(2,1)S(1)}, u32[]{:S(2)}, u32[]{:S(2)}) async-start(bf16[8,32,512]{2,1,0:T(8,128)(2,1)} %bitcast.17), calls=%async_computation.2 | async-start | bytes 524288 | tf_op jit(solution)/shard_map/all_to_all | solution.py:323
  159.0 0.1 pad_add_fusion.place_ref
  159.1 0.0 collective-permute-done.7.other_ref
  159.1 2.0 %assemble.1 = (bf16[256,2048]{1,0:T(8,128)(2,1)}, bf16[256,2048]{1,0:T(8,128)(2,1)}) custom-call(s32[2]{0:T(128)S(1)} %pad_add_fusion.place_ref, bf16[4,2,32,2048]{3,2,1,0:T(8,128)(2,1)S(1)} %pad_maximum_fusion.mine_ref, bf16[4,2,32,2048]{3,2,1,0:T(8,128)(2,1)S(1)} %collective-permute-done.7.other_ref), custom_call_target="tpu_custom_call" | custom-call | tf_op jit(solution)/shard_map/assemble/pallas_call | solution.py:275
  161.1 7.6 %all-to-all-done.2 = bf16[8,32,512]{2,1,0:T(8,128)(2,1)S(1)} async-done(((bf16[8,32,512]{2,1,0:T(8,128)(2,1)}), bf16[8,32,512]{2,1,0:T(8,128)(2,1)S(1)}, u32[]{:S(2)}, u32[]{:S(2)}) %all-to-all-start.2) | async-done | bytes 262176 | tf_op jit(solution)/shard_map/all_to_all | solution.py:323
  168.7 0.0 copy-done.5
  168.7 0.6 bitcast_add_fusion.1
  (1 shorter events, 0.0 us)
Async XLA Ops:
  7.2 30.1 %copy-start = (f32[3,4096]{1,0:T(4,128)S(1)}, f32[3,4096]{1,0:T(4,128)}, u32[]{:S(2)}) copy-start(f32[3,4096]{1,0:T(4,128)} %param.15) | copy-start | bytes 147460
  7.2 26.8 %copy-start.4 = (bf16[256,2048]{1,0:T(8,128)(2,1)S(1)}, bf16[256,2048]{1,0:T(8,128)(2,1)}, u32[]{:S(2)}) copy-start(bf16[256,2048]{1,0:T(8,128)(2,1)} %cot_hbm.1) | copy-start | bytes 3145732
  7.2 71.9 %all-gather.3.cloned.1.call-start = ((), (), s32[]{:S(2)}) async-start(), calls=%async_computation.3 | async-start | bytes 7077888 | tf_op jit(solution)/shard_map/all_gather | solution.py:313
  86.7 4.4 %copy-start.1 = (f32[3,512]{1,0:T(4,128)S(1)}, f32[3,512]{1,0:T(4,128)}, u32[]{:S(2)}) copy-start(f32[3,512]{1,0:T(4,128)} %constant_dynamic-slice_fusion.taps_ref) | copy-start | bytes 18436
  86.7 4.4 %copy-start.2 = (f32[512]{0:T(512)S(1)}, f32[512]{0:T(512)}, u32[]{:S(2)}) copy-start(f32[512]{0:T(512)} %dynamic_slice.32) | copy-start | bytes 6148
  86.7 4.4 %copy-start.3 = (s32[2]{0:T(128)S(1)}, s32[2]{0:T(128)}, u32[]{:S(2)}) copy-start(s32[2]{0:T(128)} %pad_add_fusion.1.stride_ref) | copy-start | bytes 28
  86.7 62.8 %all-to-all-start.1 = ((bf16[8,256,512]{2,1,0:T(8,128)(2,1)}), bf16[8,256,512]{2,1,0:T(8,128)(2,1)}, u32[]{:S(2)}, u32[]{:S(2)}) async-start(bf16[8,256,512]{2,1,0:T(8,128)(2,1)} %bitcast.32), calls=%async_computation.1 | async-start | bytes 4194304 | tf_op jit(solution)/shard_map/all_to_all | solution.py:319
  100.7 6.2 %collective-permute-start = (bf16[4,2,32,2048]{3,2,1,0:T(8,128)(2,1)S(1)}, bf16[4,2,32,2048]{3,2,1,0:T(8,128)(2,1)S(1)}, u32[]{:S(2)}, u32[]{:S(2)}) collective-permute-start(bf16[4,2,32,2048]{3,2,1,0:T(8,128)(2,1)S(1)} %get-tuple-element.13), channel_id=1, source_target_pairs={{0,1},{1,0},{2,3},{3,2},{4,5},{5,4},{6,7},{7,6},{8,9},{9,8},{10,11... | collective-permute-start | bytes 3145736 | tf_op jit(solution)/shard_map/ppermute | solution.py:287
  107.2 10.7 %collective-permute-start.1 = (bf16[2,32,2048]{2,1,0:T(8,128)(2,1)S(1)}, bf16[2,32,2048]{2,1,0:T(8,128)(2,1)S(1)}, u32[]{:S(2)}, u32[]{:S(2)}) collective-permute-start(bf16[2,32,2048]{2,1,0:T(8,128)(2,1)S(1)} %get-tuple-element.17), channel_id=1, source_target_pairs={{0,2},{2,4},{4,6},{6,0},{1,3},{3,5},{5,7},{7,1},{8,10},{10,12},{12... | collective-permute-start | bytes 786440 | tf_op jit(solution)/shard_map/ppermute | solution.py:291
  110.3 14.0 %collective-permute-start.2 = (bf16[2,32,2048]{2,1,0:T(8,128)(2,1)S(1)}, bf16[2,32,2048]{2,1,0:T(8,128)(2,1)S(1)}, u32[]{:S(2)}, u32[]{:S(2)}) collective-permute-start(bf16[2,32,2048]{2,1,0:T(8,128)(2,1)S(1)} %get-tuple-element.19), channel_id=1, source_target_pairs={{0,4},{2,6},{4,0},{6,2},{1,5},{3,7},{5,1},{7,3},{8,12},{10,14},{12... | collective-permute-start | bytes 786440 | tf_op jit(solution)/shard_map/ppermute | solution.py:291
  114.6 11.1 %collective-permute-start.3 = (bf16[2,32,2048]{2,1,0:T(8,128)(2,1)S(1)}, bf16[2,32,2048]{2,1,0:T(8,128)(2,1)}, u32[]{:S(2)}, u32[]{:S(2)}) collective-permute-start(bf16[2,32,2048]{2,1,0:T(8,128)(2,1)S(1)} %get-tuple-element.18), channel_id=1, source_target_pairs={{0,6},{2,0},{4,2},{6,4},{1,7},{3,1},{5,3},{7,5},{8,14},{10,8},{12,... | collective-permute-start | bytes 786440 | tf_op jit(solution)/shard_map/ppermute | solution.py:291
  126.8 11.3 %collective-permute-start.4 = (bf16[2,32,2048]{2,1,0:T(8,128)(2,1)S(1)}, bf16[2,32,2048]{2,1,0:T(8,128)(2,1)S(1)}, u32[]{:S(2)}, u32[]{:S(2)}) collective-permute-start(bf16[2,32,2048]{2,1,0:T(8,128)(2,1)S(1)} %fusion.2), channel_id=1, source_target_pairs={{0,2},{2,4},{4,6},{6,0},{1,3},{3,5},{5,7},{7,1},{8,10},{10,12},{12... | collective-permute-start | bytes 786440 | tf_op jit(solution)/shard_map/ppermute | solution.py:291
  131.8 12.6 %collective-permute-start.5 = (bf16[2,32,2048]{2,1,0:T(8,128)(2,1)S(1)}, bf16[2,32,2048]{2,1,0:T(8,128)(2,1)S(1)}, u32[]{:S(2)}, u32[]{:S(2)}) collective-permute-start(bf16[2,32,2048]{2,1,0:T(8,128)(2,1)S(1)} %fusion.2), channel_id=1, source_target_pairs={{0,4},{2,6},{4,0},{6,2},{1,5},{3,7},{5,1},{7,3},{8,12},{10,14},{12... | collective-permute-start | bytes 786440 | tf_op jit(solution)/shard_map/ppermute | solution.py:291
  135.0 10.2 %collective-permute-start.6 = (bf16[2,32,2048]{2,1,0:T(8,128)(2,1)S(1)}, bf16[2,32,2048]{2,1,0:T(8,128)(2,1)S(1)}, u32[]{:S(2)}, u32[]{:S(2)}) collective-permute-start(bf16[2,32,2048]{2,1,0:T(8,128)(2,1)S(1)} %fusion.2), channel_id=1, source_target_pairs={{0,6},{2,0},{4,2},{6,4},{1,7},{3,1},{5,3},{7,5},{8,14},{10,8},{12,... | collective-permute-start | bytes 786440 | tf_op jit(solution)/shard_map/ppermute | solution.py:291
  145.4 23.3 %copy-start.5 = (f32[512,32]{0,1:T(8,128)S(1)}, f32[512,32]{0,1:T(8,128)}, u32[]{:S(2)}) copy-start(f32[512,32]{0,1:T(8,128)} %param.17) | copy-start | bytes 196612
  145.4 13.7 %collective-permute-start.7 = (bf16[4,2,32,2048]{3,2,1,0:T(8,128)(2,1)S(1)}, bf16[4,2,32,2048]{3,2,1,0:T(8,128)(2,1)S(1)}, u32[]{:S(2)}, u32[]{:S(2)}) collective-permute-start(bf16[4,2,32,2048]{3,2,1,0:T(8,128)(2,1)S(1)} %pad_maximum_fusion.mine_ref), channel_id=1, source_target_pairs={{0,1},{1,0},{2,3},{3,2},{4,5},{5,4},{6,7},{7,6},{8,9},{9,8},{10,11... | collective-permute-start | bytes 3145736 | tf_op jit(solution)/shard_map/ppermute | solution.py:287
  152.1 16.5 %all-to-all-start.2 = ((bf16[8,32,512]{2,1,0:T(8,128)(2,1)}), bf16[8,32,512]{2,1,0:T(8,128)(2,1)S(1)}, u32[]{:S(2)}, u32[]{:S(2)}) async-start(bf16[8,32,512]{2,1,0:T(8,128)(2,1)} %bitcast.17), calls=%async_computation.2 | async-start | bytes 524288 | tf_op jit(solution)/shard_map/all_to_all | solution.py:323
Sparse Core Ops, SparseCore 0:
  34.0 45.0 all-gather.2

commit v4 on v0

--- a/solution.py
+++ b/solution.py
@@ -275,13 +275,13 @@
         return left.astype(jnp.float32) + right.astype(jnp.float32)
 
     total = chip_piece(x)
-    for d in (2, 1, 3):
+    for d in range(1, NX):
         sent = chip_piece(lax.rem(x + d, NX)).astype(jnp.bfloat16)
         arrived = moved(sent, d)
         total = total + arrived.astype(jnp.float32)
     total = total.astype(jnp.bfloat16)
-    spread = {d: moved(total, d) for d in (2, 1, 3)}
-    mine = jnp.stack([total] + [spread[d] for d in range(1, NX)])
+    spread = [moved(total, d) for d in range(1, NX)]
+    mine = jnp.stack([total] + spread)
     other = exchanged(mine)
     where = jnp.stack([x, core]).astype(jnp.int32)
     y_late, dx_early = assemble(where, mine, other)

time: 173 us -> 176 us (1.017)
  waiting for transfers between devices: 73.4 us -> 77.9 us
  starting transfers between devices: 36.7 us -> 34.4 us
    ppermute x6, waiting for transfers between devices: 19.8 us -> 24.3 us  [moved(): return lax.ppermute(value, 'x', [(i, (i + steps) % NX) for i in range(NX)])]
  transfers between devices with their start and end apart: 11 -> 11, of which waited for: 7 -> 9; matrix products, arithmetic and copies ran while one was open for 3% -> 3% of each run, Pallas kernels for 1% -> 1%
where the time goes in v4:
time: 176 us; the launch traced here: 175 us
  waiting for transfers between devices  77.9 us (44%)
  starting transfers between devices  34.4 us (20%)
  blocking collectives  25.7 us (15%)
  Pallas kernels  15.4 us (9%)
  between operations  14.2 us (8%)
  other arithmetic  5.89 us (3%)
    all_gather x1, waiting for transfers between devices, shards(): w = lax.all_gather(near, AXES, axis_index_groups=SECOND)  43.8 us
    all_to_all x1, blocking collectives, shards(): lax.all_to_all(jnp.broadcast_to(mine[None], (8,) + mine.shape), AXES, 0,...  25.7 us
    ppermute x6, waiting for transfers between devices, moved(): return lax.ppermute(value, 'x', [(i, (i + steps) % NX) for i in range(NX)])  24.3 us
    ppermute x6, starting transfers between devices, moved(): return lax.ppermute(value, 'x', [(i, (i + steps) % NX) for i in range(NX)])  16.5 us
    pallas_call x1, Pallas kernels, layer(): pl.pallas_call(layer_kernel, out_shape=(piece, piece, jax.ShapeDtypeStruc...  10.8 us
    all_to_all x1, waiting for transfers between devices, shards(): grad = lax.all_to_all(grad, AXES, 0, 0, tiled=True, axis_index_groups=FIRST)  7.56 us
    all_to_all x1, starting transfers between devices, shards(): grad = lax.all_to_all(grad, AXES, 0, 0, tiled=True, axis_index_groups=FIRST)  6.9 us
    ppermute x2, starting transfers between devices, exchanged(): return lax.ppermute(value, 'c', [(0, 1), (1, 0)])  6.48 us
  transfers between devices with their start and end apart: 11, of which 9 were waited for; matrix products, arithmetic and copies ran while one was open for 3% of the time, Pallas kernels for 1%

profile of v4, /device:TPU:1, one launch (start us, length us, event | category | flops | bytes accessed | tf_op | source)
XLA Modules:
  0.0 174.9 jit_solution(7472472004187565034)
XLA Ops:
  7.2 0.0 copy-start
  7.2 0.0 copy-start.1
  7.2 0.0 all-gather.3.cloned.1.call-start
  7.2 0.9 pad_maximum_fusion.1
  8.1 0.1 broadcast_in_dim.10
  8.2 25.7 %all_to_all.15 = bf16[8,32,1536]{2,1,0:T(8,128)(2,1)} all-to-all(bf16[8,32,1536]{2,1,0:T(8,128)(2,1)S(1)} %broadcast_in_dim.10), channel_id=1, replica_groups={{0,8,16,24,32,40,48,56},{1,65,129,193,257,321,385,449},{64,72,80,88,96,..., dimensions={0} | all-to-all | bytes 1572864 | tf_op jit(solution)/shard_map/all_to_all | solution.py:252
  33.9 0.0 all-gather.3.cloned.1.call-update
  33.9 0.0 copy-done.1
  33.9 0.5 copy.14
  34.5 0.8 dynamic_slice.32
  35.2 0.1 pad_add_fusion.1.stride_ref
  35.3 0.0 copy-done
  35.3 43.8 %all-gather.3.cloned.1.call-done = bf16[64,32,1536]{2,1,0:T(8,128)(2,1)} async-done(((bf16[8,32,1536]{2,1,0:T(8,128)(2,1)}), bf16[64,32,1536]{2,1,0:T(8,128)(2,1)}) %all-gather.3.cloned.1.call-update) | async-done | bytes 6291472 | tf_op jit(solution)/shard_map/all_gather | solution.py:256
  79.1 10.8 %layer.1 = (bf16[4,2,32,2048]{3,2,1,0:T(8,128)(2,1)S(1)}, bf16[4,2,32,2048]{3,2,1,0:T(8,128)(2,1)S(1)}, bf16[256,512]{1,0:T(8,128)(2,1)S(1)}) custom-call(s32[2]{0:T(128)S(1)} %pad_add_fusion.1.stride_ref, f32[3,512]{1,0:T(4,128)S(1)} %constant_dynamic-slice_fusion.taps_ref, f32[1,512]{1,0:T(1,128)S(1)} %bitcast.31, bf16[256,2048]{1,0:T(8,128)(2,1)} %xe_hbm.1, ...), custom_call_target="tpu_custom_call" | custom-call | flops 6000000000 | bytes 12000000 | tf_op jit(solution)/shard_map/layer/pallas_call | solution.py:152
  90.0 0.0 copy-start.2
  90.0 2.6 %gradient.1 = bf16[2048,512]{1,0:T(8,128)(2,1)} custom-call(s32[2]{0:T(128)S(1)} %pad_add_fusion.1.stride_ref, bf16[2048,256]{1,0:T(8,128)(2,1)S(1)} %bitcast.30, bf16[256,512]{1,0:T(8,128)(2,1)S(1)} %get-tuple-element.12.hidden_ref), custom_call_target="tpu_custom_call" | custom-call | flops 1000000000 | bytes 4000000 | tf_op jit(solution)/shard_map/gradient/pallas_call | solution.py:187
  92.5 0.0 copy-done.2
  92.5 0.0 copy-start.3
  92.5 4.5 %all-to-all-start.1 = ((bf16[8,256,512]{2,1,0:T(8,128)(2,1)}), bf16[8,256,512]{2,1,0:T(8,128)(2,1)}, u32[]{:S(2)}, u32[]{:S(2)}) async-start(bf16[8,256,512]{2,1,0:T(8,128)(2,1)} %bitcast.16), calls=%async_computation.1 | async-start | bytes 4194304 | tf_op jit(solution)/shard_map/all_to_all | solution.py:263
  97.0 0.0 copy-done.3
  97.0 3.9 %collective-permute-start = (bf16[4,2,32,2048]{3,2,1,0:T(8,128)(2,1)S(1)}, bf16[4,2,32,2048]{3,2,1,0:T(8,128)(2,1)S(1)}, u32[]{:S(2)}, u32[]{:S(2)}) collective-permute-start(bf16[4,2,32,2048]{3,2,1,0:T(8,128)(2,1)S(1)} %copy-done.3), channel_id=1, source_target_pairs={{0,1},{1,0},{2,3},{3,2},{4,5},{5,4},{6,7},{7,6},{8,9},{9,8},{10,11... | collective-permute-start | bytes 3145736 | tf_op jit(solution)/shard_map/ppermute | solution.py:234
  101.0 2.2 %collective-permute-done = bf16[4,2,32,2048]{3,2,1,0:T(8,128)(2,1)S(1)} collective-permute-done((bf16[4,2,32,2048]{3,2,1,0:T(8,128)(2,1)S(1)}, bf16[4,2,32,2048]{3,2,1,0:T(8,128)(2,1)S(1)}, u32[]{:S(2)}, u32[]{:S(2)}) %collective-permute-start) | collective-permute-done | bytes 1048608 | tf_op jit(solution)/shard_map/ppermute | solution.py:234
  103.3 0.3 fusion.3
  103.5 4.3 %collective-permute-start.3 = (bf16[2,32,2048]{2,1,0:T(8,128)(2,1)S(1)}, bf16[2,32,2048]{2,1,0:T(8,128)(2,1)S(1)}, u32[]{:S(2)}, u32[]{:S(2)}) collective-permute-start(bf16[2,32,2048]{2,1,0:T(8,128)(2,1)S(1)} %get-tuple-element.14), channel_id=1, source_target_pairs={{0,6},{2,0},{4,2},{6,4},{1,7},{3,1},{5,3},{7,5},{8,14},{10,8},{12,... | collective-permute-start | bytes 786440 | tf_op jit(solution)/shard_map/ppermute | solution.py:238
  107.8 2.5 %collective-permute-start.2 = (bf16[2,32,2048]{2,1,0:T(8,128)(2,1)S(1)}, bf16[2,32,2048]{2,1,0:T(8,128)(2,1)S(1)}, u32[]{:S(2)}, u32[]{:S(2)}) collective-permute-start(bf16[2,32,2048]{2,1,0:T(8,128)(2,1)S(1)} %get-tuple-element.15), channel_id=1, source_target_pairs={{0,4},{2,6},{4,0},{6,2},{1,5},{3,7},{5,1},{7,3},{8,12},{10,14},{12... | collective-permute-start | bytes 786440 | tf_op jit(solution)/shard_map/ppermute | solution.py:238
  110.3 2.5 %collective-permute-start.1 = (bf16[2,32,2048]{2,1,0:T(8,128)(2,1)S(1)}, bf16[2,32,2048]{2,1,0:T(8,128)(2,1)}, u32[]{:S(2)}, u32[]{:S(2)}) collective-permute-start(bf16[2,32,2048]{2,1,0:T(8,128)(2,1)S(1)} %get-tuple-element.13), channel_id=1, source_target_pairs={{0,2},{2,4},{4,6},{6,0},{1,3},{3,5},{5,7},{7,1},{8,10},{10,12},{12... | collective-permute-start | bytes 786440 | tf_op jit(solution)/shard_map/ppermute | solution.py:238
  112.8 1.0 collective-permute-done.3
  113.8 4.7 %collective-permute-done.2 = bf16[2,32,2048]{2,1,0:T(8,128)(2,1)S(1)} collective-permute-done((bf16[2,32,2048]{2,1,0:T(8,128)(2,1)S(1)}, bf16[2,32,2048]{2,1,0:T(8,128)(2,1)S(1)}, u32[]{:S(2)}, u32[]{:S(2)}) %collective-permute-start.2) | collective-permute-done | bytes 262176 | tf_op jit(solution)/shard_map/ppermute | solution.py:238
  118.5 6.7 %collective-permute-done.1 = bf16[2,32,2048]{2,1,0:T(8,128)(2,1)} collective-permute-done((bf16[2,32,2048]{2,1,0:T(8,128)(2,1)S(1)}, bf16[2,32,2048]{2,1,0:T(8,128)(2,1)}, u32[]{:S(2)}, u32[]{:S(2)}) %collective-permute-start.1) | collective-permute-done | bytes 262176 | tf_op jit(solution)/shard_map/ppermute | solution.py:238
  125.2 1.1 fusion.2
  126.3 1.9 %collective-permute-start.6 = (bf16[2,32,2048]{2,1,0:T(8,128)(2,1)S(1)}, bf16[2,32,2048]{2,1,0:T(8,128)(2,1)S(1)}, u32[]{:S(2)}, u32[]{:S(2)}) collective-permute-start(bf16[2,32,2048]{2,1,0:T(8,128)(2,1)S(1)} %fusion.2), channel_id=1, source_target_pairs={{0,6},{2,0},{4,2},{6,4},{1,7},{3,1},{5,3},{7,5},{8,14},{10,8},{12,... | collective-permute-start | bytes 786440 | tf_op jit(solution)/shard_map/ppermute | solution.py:238
  128.2 2.5 %collective-permute-start.5 = (bf16[2,32,2048]{2,1,0:T(8,128)(2,1)S(1)}, bf16[2,32,2048]{2,1,0:T(8,128)(2,1)S(1)}, u32[]{:S(2)}, u32[]{:S(2)}) collective-permute-start(bf16[2,32,2048]{2,1,0:T(8,128)(2,1)S(1)} %fusion.2), channel_id=1, source_target_pairs={{0,4},{2,6},{4,0},{6,2},{1,5},{3,7},{5,1},{7,3},{8,12},{10,14},{12... | collective-permute-start | bytes 786440 | tf_op jit(solution)/shard_map/ppermute | solution.py:238
  130.7 2.8 %collective-permute-start.4 = (bf16[2,32,2048]{2,1,0:T(8,128)(2,1)S(1)}, bf16[2,32,2048]{2,1,0:T(8,128)(2,1)S(1)}, u32[]{:S(2)}, u32[]{:S(2)}) collective-permute-start(bf16[2,32,2048]{2,1,0:T(8,128)(2,1)S(1)} %fusion.2), channel_id=1, source_target_pairs={{0,2},{2,4},{4,6},{6,0},{1,3},{3,5},{5,7},{7,1},{8,10},{10,12},{12... | collective-permute-start | bytes 786440 | tf_op jit(solution)/shard_map/ppermute | solution.py:238
  133.5 2.0 %collective-permute-done.6 = bf16[2,32,2048]{2,1,0:T(8,128)(2,1)S(1)} collective-permute-done((bf16[2,32,2048]{2,1,0:T(8,128)(2,1)S(1)}, bf16[2,32,2048]{2,1,0:T(8,128)(2,1)S(1)}, u32[]{:S(2)}, u32[]{:S(2)}) %collective-permute-start.6) | collective-permute-done | bytes 262176 | tf_op jit(solution)/shard_map/ppermute | solution.py:238
  135.6 2.8 %collective-permute-done.5 = bf16[2,32,2048]{2,1,0:T(8,128)(2,1)S(1)} collective-permute-done((bf16[2,32,2048]{2,1,0:T(8,128)(2,1)S(1)}, bf16[2,32,2048]{2,1,0:T(8,128)(2,1)S(1)}, u32[]{:S(2)}, u32[]{:S(2)}) %collective-permute-start.5) | collective-permute-done | bytes 262176 | tf_op jit(solution)/shard_map/ppermute | solution.py:238
  138.4 7.1 %collective-permute-done.4 = bf16[2,32,2048]{2,1,0:T(8,128)(2,1)S(1)} collective-permute-done((bf16[2,32,2048]{2,1,0:T(8,128)(2,1)S(1)}, bf16[2,32,2048]{2,1,0:T(8,128)(2,1)S(1)}, u32[]{:S(2)}, u32[]{:S(2)}) %collective-permute-start.4) | collective-permute-done | bytes 262176 | tf_op jit(solution)/shard_map/ppermute | solution.py:238
  145.5 0.1 pad_maximum_fusion.mine_ref
  145.6 0.0 copy-start.4
  145.6 2.5 %collective-permute-start.7 = (bf16[4,2,32,2048]{3,2,1,0:T(8,128)(2,1)S(1)}, bf16[4,2,32,2048]{3,2,1,0:T(8,128)(2,1)S(1)}, u32[]{:S(2)}, u32[]{:S(2)}) collective-permute-start(bf16[4,2,32,2048]{3,2,1,0:T(8,128)(2,1)S(1)} %pad_maximum_fusion.mine_ref), channel_id=1, source_target_pairs={{0,1},{1,0},{2,3},{3,2},{4,5},{5,4},{6,7},{7,6},{8,9},{9,8},{10,11... | collective-permute-start | bytes 3145736 | tf_op jit(solution)/shard_map/ppermute | solution.py:234
  148.2 0.0 all-to-all-done.1
  148.2 2.7 %reduce_sum.21 = bf16[256,512]{1,0:T(8,128)(2,1)} reduce(bf16[8,256,512]{2,1,0:T(8,128)(2,1)} %all-to-all-done.1, bf16[]{:T(256)} %constant.52.clone.1), dimensions={0}, to_apply=%region_0.0 | reduce | flops 917504 | bytes 2359298 | tf_op jit(solution)/shard_map/reduce_sum | solution.py:242
  150.9 6.9 %all-to-all-start.2 = ((bf16[8,32,512]{2,1,0:T(8,128)(2,1)}), bf16[8,32,512]{2,1,0:T(8,128)(2,1)S(1)}, u32[]{:S(2)}, u32[]{:S(2)}) async-start(bf16[8,32,512]{2,1,0:T(8,128)(2,1)} %bitcast.17), calls=%async_computation.2 | async-start | bytes 524288 | tf_op jit(solution)/shard_map/all_to_all | solution.py:267
  157.8 0.1 pad_add_fusion.place_ref
  157.8 0.0 collective-permute-done.7.other_ref
  157.8 2.0 %assemble.1 = (bf16[256,2048]{1,0:T(8,128)(2,1)}, bf16[256,2048]{1,0:T(8,128)(2,1)}) custom-call(s32[2]{0:T(128)S(1)} %pad_add_fusion.place_ref, bf16[4,2,32,2048]{3,2,1,0:T(8,128)(2,1)S(1)} %pad_maximum_fusion.mine_ref, bf16[4,2,32,2048]{3,2,1,0:T(8,128)(2,1)S(1)} %collective-permute-done.7.other_ref), custom_call_target="tpu_custom_call" | custom-call | tf_op jit(solution)/shard_map/assemble/pallas_call | solution.py:222
  159.8 7.6 %all-to-all-done.2 = bf16[8,32,512]{2,1,0:T(8,128)(2,1)S(1)} async-done(((bf16[8,32,512]{2,1,0:T(8,128)(2,1)}), bf16[8,32,512]{2,1,0:T(8,128)(2,1)S(1)}, u32[]{:S(2)}, u32[]{:S(2)}) %all-to-all-start.2) | async-done | bytes 262176 | tf_op jit(solution)/shard_map/all_to_all | solution.py:267
  167.4 0.0 copy-done.4
  167.4 0.6 bitcast_add_fusion.1
  (2 shorter events, 0.0 us)
Async XLA Ops:
  7.2 28.2 %copy-start = (f32[3,4096]{1,0:T(4,128)S(1)}, f32[3,4096]{1,0:T(4,128)}, u32[]{:S(2)}) copy-start(f32[3,4096]{1,0:T(4,128)} %param.15) | copy-start | bytes 147460
  7.2 26.8 %copy-start.1 = (bf16[256,2048]{1,0:T(8,128)(2,1)S(1)}, bf16[256,2048]{1,0:T(8,128)(2,1)}, u32[]{:S(2)}) copy-start(bf16[256,2048]{1,0:T(8,128)(2,1)} %cot_ref.1) | copy-start | bytes 3145732
  7.2 71.9 %all-gather.3.cloned.1.call-start = ((), (), s32[]{:S(2)}) async-start(), calls=%async_computation.3 | async-start | bytes 7077888 | tf_op jit(solution)/shard_map/all_gather | solution.py:256
  90.0 2.6 %copy-start.2 = (bf16[4,2,32,2048]{3,2,1,0:T(8,128)(2,1)}, bf16[4,2,32,2048]{3,2,1,0:T(8,128)(2,1)S(1)}, u32[]{:S(2)}) copy-start(bf16[4,2,32,2048]{3,2,1,0:T(8,128)(2,1)S(1)} %get-tuple-element.9) | copy-start | bytes 3145732
  92.5 4.5 %copy-start.3 = (bf16[4,2,32,2048]{3,2,1,0:T(8,128)(2,1)S(1)}, bf16[4,2,32,2048]{3,2,1,0:T(8,128)(2,1)}, u32[]{:S(2)}) copy-start(bf16[4,2,32,2048]{3,2,1,0:T(8,128)(2,1)} %copy-done.2) | copy-start | bytes 3145732
  92.5 55.6 %all-to-all-start.1 = ((bf16[8,256,512]{2,1,0:T(8,128)(2,1)}), bf16[8,256,512]{2,1,0:T(8,128)(2,1)}, u32[]{:S(2)}, u32[]{:S(2)}) async-start(bf16[8,256,512]{2,1,0:T(8,128)(2,1)} %bitcast.16), calls=%async_computation.1 | async-start | bytes 4194304 | tf_op jit(solution)/shard_map/all_to_all | solution.py:263
  97.0 6.2 %collective-permute-start = (bf16[4,2,32,2048]{3,2,1,0:T(8,128)(2,1)S(1)}, bf16[4,2,32,2048]{3,2,1,0:T(8,128)(2,1)S(1)}, u32[]{:S(2)}, u32[]{:S(2)}) collective-permute-start(bf16[4,2,32,2048]{3,2,1,0:T(8,128)(2,1)S(1)} %copy-done.3), channel_id=1, source_target_pairs={{0,1},{1,0},{2,3},{3,2},{4,5},{5,4},{6,7},{7,6},{8,9},{9,8},{10,11... | collective-permute-start | bytes 3145736 | tf_op jit(solution)/shard_map/ppermute | solution.py:234
  103.5 10.3 %collective-permute-start.3 = (bf16[2,32,2048]{2,1,0:T(8,128)(2,1)S(1)}, bf16[2,32,2048]{2,1,0:T(8,128)(2,1)S(1)}, u32[]{:S(2)}, u32[]{:S(2)}) collective-permute-start(bf16[2,32,2048]{2,1,0:T(8,128)(2,1)S(1)} %get-tuple-element.14), channel_id=1, source_target_pairs={{0,6},{2,0},{4,2},{6,4},{1,7},{3,1},{5,3},{7,5},{8,14},{10,8},{12,... | collective-permute-start | bytes 786440 | tf_op jit(solution)/shard_map/ppermute | solution.py:238
  107.8 10.6 %collective-permute-start.2 = (bf16[2,32,2048]{2,1,0:T(8,128)(2,1)S(1)}, bf16[2,32,2048]{2,1,0:T(8,128)(2,1)S(1)}, u32[]{:S(2)}, u32[]{:S(2)}) collective-permute-start(bf16[2,32,2048]{2,1,0:T(8,128)(2,1)S(1)} %get-tuple-element.15), channel_id=1, source_target_pairs={{0,4},{2,6},{4,0},{6,2},{1,5},{3,7},{5,1},{7,3},{8,12},{10,14},{12... | collective-permute-start | bytes 786440 | tf_op jit(solution)/shard_map/ppermute | solution.py:238
  110.3 14.9 %collective-permute-start.1 = (bf16[2,32,2048]{2,1,0:T(8,128)(2,1)S(1)}, bf16[2,32,2048]{2,1,0:T(8,128)(2,1)}, u32[]{:S(2)}, u32[]{:S(2)}) collective-permute-start(bf16[2,32,2048]{2,1,0:T(8,128)(2,1)S(1)} %get-tuple-element.13), channel_id=1, source_target_pairs={{0,2},{2,4},{4,6},{6,0},{1,3},{3,5},{5,7},{7,1},{8,10},{10,12},{12... | collective-permute-start | bytes 786440 | tf_op jit(solution)/shard_map/ppermute | solution.py:238
  126.3 9.3 %collective-permute-start.6 = (bf16[2,32,2048]{2,1,0:T(8,128)(2,1)S(1)}, bf16[2,32,2048]{2,1,0:T(8,128)(2,1)S(1)}, u32[]{:S(2)}, u32[]{:S(2)}) collective-permute-start(bf16[2,32,2048]{2,1,0:T(8,128)(2,1)S(1)} %fusion.2), channel_id=1, source_target_pairs={{0,6},{2,0},{4,2},{6,4},{1,7},{3,1},{5,3},{7,5},{8,14},{10,8},{12,... | collective-permute-start | bytes 786440 | tf_op jit(solution)/shard_map/ppermute | solution.py:238
  128.2 10.2 %collective-permute-start.5 = (bf16[2,32,2048]{2,1,0:T(8,128)(2,1)S(1)}, bf16[2,32,2048]{2,1,0:T(8,128)(2,1)S(1)}, u32[]{:S(2)}, u32[]{:S(2)}) collective-permute-start(bf16[2,32,2048]{2,1,0:T(8,128)(2,1)S(1)} %fusion.2), channel_id=1, source_target_pairs={{0,4},{2,6},{4,0},{6,2},{1,5},{3,7},{5,1},{7,3},{8,12},{10,14},{12... | collective-permute-start | bytes 786440 | tf_op jit(solution)/shard_map/ppermute | solution.py:238
  130.7 14.8 %collective-permute-start.4 = (bf16[2,32,2048]{2,1,0:T(8,128)(2,1)S(1)}, bf16[2,32,2048]{2,1,0:T(8,128)(2,1)S(1)}, u32[]{:S(2)}, u32[]{:S(2)}) collective-permute-start(bf16[2,32,2048]{2,1,0:T(8,128)(2,1)S(1)} %fusion.2), channel_id=1, source_target_pairs={{0,2},{2,4},{4,6},{6,0},{1,3},{3,5},{5,7},{7,1},{8,10},{10,12},{12... | collective-permute-start | bytes 786440 | tf_op jit(solution)/shard_map/ppermute | solution.py:238
  145.6 21.8 %copy-start.4 = (f32[512,32]{0,1:T(8,128)S(1)}, f32[512,32]{0,1:T(8,128)}, u32[]{:S(2)}) copy-start(f32[512,32]{0,1:T(8,128)} %param.17) | copy-start | bytes 196612
  145.6 12.2 %collective-permute-start.7 = (bf16[4,2,32,2048]{3,2,1,0:T(8,128)(2,1)S(1)}, bf16[4,2,32,2048]{3,2,1,0:T(8,128)(2,1)S(1)}, u32[]{:S(2)}, u32[]{:S(2)}) collective-permute-start(bf16[4,2,32,2048]{3,2,1,0:T(8,128)(2,1)S(1)} %pad_maximum_fusion.mine_ref), channel_id=1, source_target_pairs={{0,1},{1,0},{2,3},{3,2},{4,5},{5,4},{6,7},{7,6},{8,9},{9,8},{10,11... | collective-permute-start | bytes 3145736 | tf_op jit(solution)/shard_map/ppermute | solution.py:234
  150.9 16.5 %all-to-all-start.2 = ((bf16[8,32,512]{2,1,0:T(8,128)(2,1)}), bf16[8,32,512]{2,1,0:T(8,128)(2,1)S(1)}, u32[]{:S(2)}, u32[]{:S(2)}) async-start(bf16[8,32,512]{2,1,0:T(8,128)(2,1)} %bitcast.17), calls=%async_computation.2 | async-start | bytes 524288 | tf_op jit(solution)/shard_map/all_to_all | solution.py:267
Sparse Core Ops, SparseCore 0:
  34.0 45.0 all-gather.2
